TPU v7x, 512 devices: a whole 4x4x16 slice. The times are simulated.
512 devices in a mesh: sp: 32 (over z, core), tp: 16 (over y, x).
Axes of the slice: x: 4, y: 4, z: 16, core: 2. Of those that a mesh axis runs over, the one named last changes fastest.
Arguments:
- queries: bfloat16 [8192, 2048], P('sp', 'tp'), may hold values from -6 to 6
- keys: bfloat16 [8192, 1024], P('sp', 'tp'), may hold values from -6 to 6
- values: bfloat16 [8192, 1024], P('sp', 'tp'), may hold values from -6 to 6
- sink_logit: float32 [32], P('tp'), may hold values from -1 to 6
- out_weight: bfloat16 [2048, 2048], P(None, 'tp'), may hold values from -0.125 to 0.125
- residual: bfloat16 [8192, 2048], P(('sp', 'tp')), may hold values from -1.796875 to 1.796875
- norm_gain: float32 [2048], replicated, may hold values from 0.1 to 1.9
- routes: int32 [8192, 2], P(('sp', 'tp')), may hold values from 0 to 31, all different within a row; in each aligned block of 16 rows (0 to 15, 16 to 31, ...) at most 2 rows name the same one
- route_weights: float32 [8192, 2], P(('sp', 'tp')), may hold values from 0.2 to 1
- gate_weight: bfloat16 [32, 2048, 5120], P('sp', None, 'tp'), may hold values from -0.125 to 0.125
- up_weight: bfloat16 [32, 2048, 5120], P('sp', None, 'tp'), may hold values from -0.125 to 0.125
- down_weight: bfloat16 [32, 5120, 2048], P('sp', 'tp'), may hold values from -0.078125 to 0.078125
Outputs:
- mixed: bfloat16 [8192, 2048], P(('sp', 'tp'))
Inputs may be any that keep to these rules, and one draw needn't show every extreme that they name: `routes`: each row names two different experts. Among the rows of one device no expert is named more than 2 times, and in every draw some expert is named exactly 2 times by the rows of some device.
All inputs are finite; a program needn't handle non-finite values.
Results may differ from a plain program's by a relative error of at most 0.018.
Values may be sent and summed in bfloat16 or wider, within the bound.
A program may use at most 64 MiB of HBM per device.

v0:
```python
import jax
import jax.numpy as jnp
from jax import lax
from jax.sharding import PartitionSpec as P

HEADS = 32
KV_HEADS = 16
HEAD = 64
WINDOW = 128


EPS = 1e-06
NEGATIVE = -1e30


def with_halo(block, sides, width):
    for axis, dim in sides:
        count = lax.axis_size(axis)
        forward = [(i, i + 1) for i in range(count - 1)]
        backward = [(target, source) for source, target in forward]
        low = lax.ppermute(
            lax.slice_in_dim(block, block.shape[dim] - width, None, axis=dim), axis, forward
        )
        high = lax.ppermute(lax.slice_in_dim(block, 0, width, axis=dim), axis, backward)
        block = jnp.concatenate([low, block, high], axis=dim)
    return block


def sent_to_all(value, axis):
    copies = jnp.broadcast_to(value, (lax.axis_size(axis), *value.shape))
    return lax.all_to_all(copies, axis, split_axis=0, concat_axis=0, tiled=True)


def laid_out(tiles, dim):
    tiles = jnp.moveaxis(tiles, 0, dim)
    lengths = tiles.shape
    return tiles.reshape(*lengths[:dim], lengths[dim] * lengths[dim + 1], *lengths[dim + 2 :])


def gather_directly(value, axis, dim):
    tiles = sent_to_all(value, axis)
    return laid_out(tiles, dim)


def cut_along(value, dim, size):
    lengths = value.shape
    tiles = value.reshape(*lengths[:dim], size, lengths[dim] // size, *lengths[dim + 1 :])
    return jnp.moveaxis(tiles, dim, 0)


def summed_on_arrival(value, axis, dim):
    tiles = cut_along(value, dim, lax.axis_size(axis))
    arrived = lax.all_to_all(tiles, axis, split_axis=0, concat_axis=0, tiled=True)
    return arrived.astype(jnp.float32).sum(axis=0)


def make_band(extended, length):
    blocks = length // WINDOW
    pieces = [
        lax.slice_in_dim(extended, offset * WINDOW, offset * WINDOW + length, axis=0).reshape(
            blocks, WINDOW, -1
        )
        for offset in range(3)
    ]
    return jnp.concatenate(pieces, axis=1)


def attend_local(queries, keys, values, sink_logit):
    length = queries.shape[0]
    groups = keys.shape[1] // HEAD
    repeat = HEADS // KV_HEADS
    blocks = length // WINDOW
    joined = jnp.concatenate([keys, values], axis=1)
    extended = with_halo(joined, (("sp", 0),), WINDOW)
    banded = make_band(extended, length)
    key_band = banded[..., : groups * HEAD].reshape(blocks, 3 * WINDOW, groups, HEAD)
    value_band = banded[..., groups * HEAD :].reshape(blocks, 3 * WINDOW, groups, HEAD)
    query_blocks = queries.reshape(blocks, WINDOW, groups, repeat, HEAD)
    scores = jnp.einsum(
        "nqgrd,nkgd->ngrqk", query_blocks, key_band, preferred_element_type=jnp.float32
    ) * HEAD ** (-0.5)
    near = jnp.abs(jnp.arange(WINDOW)[:, None] + WINDOW - jnp.arange(3 * WINDOW)[None, :]) <= WINDOW
    first_token = lax.axis_index("sp") * length
    key_pos = (
        first_token + (jnp.arange(blocks)[:, None] - 1) * WINDOW + jnp.arange(3 * WINDOW)[None, :]
    )
    inside = (key_pos >= 0) & (key_pos < length * lax.axis_size("sp"))
    valid = near[None, None, None, :, :] & inside[:, None, None, None, :]
    sinks = sink_logit.reshape(1, groups, repeat, 1, 1)
    masked = jnp.where(valid, scores, NEGATIVE)
    top = jnp.maximum(jnp.max(masked, axis=-1, keepdims=True), sinks)
    probs = jnp.exp(masked - top)
    denom = jnp.sum(probs, axis=-1, keepdims=True) + jnp.exp(sinks - top)
    weights = (probs / denom).astype(jnp.bfloat16)
    output = jnp.einsum(
        "ngrqk,nkgd->nqgrd", weights, value_band, preferred_element_type=jnp.float32
    )
    return output.astype(jnp.bfloat16).reshape(length, groups * repeat * HEAD)


def local(
    queries,
    keys,
    values,
    sink_logit,
    out_weight,
    residual,
    norm_gain,
    routes,
    route_weights,
    gate_weight,
    up_weight,
    down_weight,
):
    attention = attend_local(queries, keys, values, sink_logit)
    columns = jnp.dot(
        gather_directly(attention, "tp", 1), out_weight, preferred_element_type=jnp.float32
    )
    projected = lax.all_to_all(
        columns.astype(jnp.bfloat16), "tp", split_axis=0, concat_axis=1, tiled=True
    )
    hidden_state = residual.astype(jnp.float32) + projected.astype(jnp.float32)
    inverse = lax.rsqrt(jnp.mean(hidden_state * hidden_state, axis=-1, keepdims=True) + EPS)
    normed = (hidden_state * inverse * norm_gain).astype(jnp.bfloat16)
    sp_count = lax.axis_size("sp")
    tok_rows = residual.shape[0]
    width = residual.shape[1]
    capacity = max(2, 4 * tok_rows // sp_count)
    slot_total = sp_count * capacity
    expert_ids = routes.reshape(-1)
    onehot = (expert_ids[:, None] == jnp.arange(sp_count, dtype=jnp.int32)[None, :]).astype(
        jnp.int32
    )
    earlier = jnp.cumsum(onehot, axis=0) - onehot
    rank = jnp.sum(earlier * onehot, axis=1)
    slots = expert_ids * capacity + rank
    placing = (slots[:, None] == jnp.arange(slot_total, dtype=jnp.int32)[None, :]).astype(
        jnp.bfloat16
    )
    placing = placing.reshape(tok_rows, 2, slot_total)
    first_place = placing[:, 0]
    second_place = placing[:, 1]
    sending = jnp.einsum(
        "ts,td->sd", first_place + second_place, normed, preferred_element_type=jnp.float32
    )
    sending = sending.astype(jnp.bfloat16).reshape(sp_count, capacity, width)
    piece = lax.all_gather(
        lax.all_to_all(sending, "sp", split_axis=0, concat_axis=0, tiled=True),
        "tp",
        axis=0,
        tiled=True,
    )
    flat = piece.reshape(-1, piece.shape[-1])
    gate = jnp.dot(flat, gate_weight[0], preferred_element_type=jnp.float32)
    upward = jnp.dot(flat, up_weight[0], preferred_element_type=jnp.float32)
    hidden = (jax.nn.silu(gate) * upward).astype(jnp.bfloat16)
    partial_value = jnp.dot(hidden, down_weight[0], preferred_element_type=jnp.float32)
    partial_value = partial_value.reshape(piece.shape[:-1] + (down_weight.shape[-1],))
    returned = lax.all_to_all(
        summed_on_arrival(partial_value.astype(jnp.bfloat16), "tp", 0).astype(jnp.bfloat16),
        "sp",
        split_axis=0,
        concat_axis=0,
        tiled=True,
    )
    gathered_back = returned.reshape(slot_total, width)
    first_pick = jnp.dot(first_place, gathered_back, preferred_element_type=jnp.float32)
    second_pick = jnp.dot(second_place, gathered_back, preferred_element_type=jnp.float32)
    mixture = route_weights[:, 0:1] * first_pick + route_weights[:, 1:2] * second_pick
    return (hidden_state + mixture).astype(jnp.bfloat16)


def solution(mesh):
    in_specs = (
        P("sp", "tp"),
        P("sp", "tp"),
        P("sp", "tp"),
        P("tp"),
        P(None, "tp"),
        P(("sp", "tp"), None),
        P(),
        P(("sp", "tp"), None),
        P(("sp", "tp"), None),
        P("sp", None, "tp"),
        P("sp", None, "tp"),
        P("sp", "tp", None),
    )
    out_specs = P(("sp", "tp"), None)
    return jax.shard_map(local, mesh=mesh, in_specs=in_specs, out_specs=out_specs, check_vma=False)
```

profile of v0, /device:TPU:1, one launch (start us, length us, event | category | flops | bytes accessed | tf_op | source)
XLA Modules:
  0.0 271.8 jit_solution(23323305794079645)
XLA Ops:
  6.5 1.0 copy.92
  7.5 0.9 copy.93
  8.4 0.1 fusion.17
  8.5 4.9 %collective-permute-start = (bf16[128,128]{1,0:T(8,128)(2,1)S(1)}, bf16[128,128]{1,0:T(8,128)(2,1)S(1)}, u32[]{:S(2)}, u32[]{:S(2)}) collective-permute-start(bf16[128,128]{1,0:T(8,128)(2,1)S(1)} %get-tuple-element.8), channel_id=1, source_target_pairs={{0,16},{16,32},{32,48},{48,64},{64,80},{80,96},{96,112},{112,128},... | collective-permute-start | bytes 98312 | tf_op jit(solution)/shard_map/ppermute | solution.py:21
  13.4 5.1 %collective-permute-start.1 = (bf16[128,128]{1,0:T(8,128)(2,1)S(1)}, bf16[128,128]{1,0:T(8,128)(2,1)S(1)}, u32[]{:S(2)}, u32[]{:S(2)}) collective-permute-start(bf16[128,128]{1,0:T(8,128)(2,1)S(1)} %get-tuple-element.9), channel_id=1, source_target_pairs={{16,0},{32,16},{48,32},{64,48},{80,64},{96,80},{112,96},{128,112},... | collective-permute-start | bytes 98312 | tf_op jit(solution)/shard_map/ppermute | solution.py:24
  18.6 0.1 abs_compare_fusion
  18.7 0.1 compare_and_fusion
  18.7 0.2 broadcast_and_fusion
  18.9 0.0 copy-start.6
  18.9 0.9 reshape.197
  19.9 0.0 collective-permute-done
  19.9 0.0 collective-permute-done.1
  19.9 0.1 pad_maximum_fusion.3
  20.0 0.1 copy.94
  20.1 0.1 copy.95
  20.3 0.1 copy.96
  20.4 0.3 fusion.24
  20.8 0.1 broadcast_maximum_fusion
  20.8 0.1 fusion.12
  21.0 0.1 exponential_add_fusion
  21.0 0.3 fusion.10
  21.3 0.1 copy.100
  21.4 1.1 broadcast_in_dim.16
  22.5 5.7 %all-to-all-start = ((bf16[16,256,128]{1,2,0:T(8,128)(2,1)}), bf16[16,256,128]{1,2,0:T(8,128)(2,1)S(1)}, u32[]{:S(2)}, u32[]{:S(2)}) async-start(bf16[16,256,128]{1,2,0:T(8,128)(2,1)} %broadcast_in_dim.16), calls=%async_computation | async-start | bytes 2097152 | tf_op jit(solution)/shard_map/all_to_all | solution.py:31
  28.2 0.0 copy-start.2
  28.2 0.0 copy-start.4
  28.2 0.1 copy.102
  28.3 0.1 eq.30
  28.4 0.1 fusion.19
  28.4 0.1 reduce_window_sum.11
  28.5 0.2 select_reduce_fusion
  28.7 0.1 reduce_sum.43
  28.8 0.1 copy.103
  28.9 15.9 %all-to-all-done = bf16[16,256,128]{1,2,0:T(8,128)(2,1)S(1)} async-done(((bf16[16,256,128]{1,2,0:T(8,128)(2,1)}), bf16[16,256,128]{1,2,0:T(8,128)(2,1)S(1)}, u32[]{:S(2)}, u32[]{:S(2)}) %all-to-all-start) | async-done | bytes 1048608 | tf_op jit(solution)/shard_map/all_to_all | solution.py:31
  44.7 1.1 convolution_convert_fusion.2
  45.8 3.5 %all-to-all-start.1 = ((bf16[16,16,128]{2,1,0:T(8,128)(2,1)}), bf16[16,16,128]{2,1,0:T(8,128)(2,1)S(1)}, u32[]{:S(2)}, u32[]{:S(2)}) async-start(bf16[16,16,128]{2,1,0:T(8,128)(2,1)} %bitcast.14), calls=%async_computation.1 | async-start | bytes 131072 | tf_op jit(solution)/shard_map/all_to_all | solution.py:119
  49.3 0.0 all-gather.2.cloned.1.call-start
  49.4 0.1 iota_compare_fusion
  49.5 6.7 %all-to-all-done.1 = bf16[16,16,128]{2,1,0:T(8,128)(2,1)S(1)} async-done(((bf16[16,16,128]{2,1,0:T(8,128)(2,1)}), bf16[16,16,128]{2,1,0:T(8,128)(2,1)S(1)}, u32[]{:S(2)}, u32[]{:S(2)}) %all-to-all-start.1) | async-done | bytes 65568 | tf_op jit(solution)/shard_map/all_to_all | solution.py:119
  56.1 0.1 multiply_reduce_fusion
  56.3 0.0 copy-done.4
  56.3 0.3 convolution_convert_fusion.1
  56.6 0.2 reshape.189
  56.8 40.8 %all_to_all.33 = bf16[32,2,2048]{2,1,0:T(2,128)(2,1)} all-to-all(bf16[32,2,2048]{2,1,0:T(2,128)(2,1)S(1)} %reshape.189), channel_id=1, replica_groups=mesh['sp'=32,'tp'=16] {'sp'}, dimensions={0} | all-to-all | bytes 524288 | tf_op jit(solution)/shard_map/all_to_all | solution.py:148
  97.6 0.0 all-gather.2.cloned.1.call-update
  97.6 0.0 copy-start.8
  97.6 54.4 %all-gather.2.cloned.1.call-done = bf16[512,2,2048]{2,1,0:T(2,128)(2,1)} async-done(((bf16[32,2,2048]{2,1,0:T(2,128)(2,1)}), bf16[512,2,2048]{2,1,0:T(2,128)(2,1)}) %all-gather.2.cloned.1.call-update) | async-done | bytes 4194320 | tf_op jit(solution)/shard_map/all_gather | solution.py:147
  152.0 7.3 %reshape.190 = bf16[1024,2048]{1,0:T(8,128)(2,1)} reshape(bf16[512,2,2048]{2,1,0:T(2,128)(2,1)} %all-gather.2.cloned.1.call-done) | data formatting | bytes 8388608 | tf_op jit(solution)/shard_map/reshape | solution.py:153
  159.3 4.0 %fusion.6 = f32[1024,320]{0,1:T(8,128)S(1)} fusion(bf16[1024,2048]{1,0:T(8,128)(2,1)} %reshape.190, bf16[1,2048,320]{1,2,0:T(8,128)(2,1)S(1)} %copy-done.8), kind=kOutput, calls=%fused_computation.11 | convolution fusion | flops 1342177280 | bytes 6815744 | tf_op jit(solution)/shard_map/dot_general | solution.py:154
  163.3 0.0 copy-done.1
  163.3 0.0 copy-done.9
  163.3 1.7 fusion.3
  165.0 0.4 copy.104
  165.4 0.3 dot_general.35
  165.7 2.3 convolution_convert_fusion
  168.1 0.6 copy.106
  168.7 54.8 %all_to_all.34 = bf16[16,32,2,2048]{3,1,2,0:T(8,128)(2,1)} all-to-all(bf16[16,32,2,2048]{3,1,2,0:T(8,128)(2,1)S(1)} %copy.106), channel_id=1, replica_groups=mesh['sp'=32,'tp'=16] {'tp'}, dimensions={0} | all-to-all | bytes 8388608 | tf_op jit(solution)/shard_map/all_to_all | solution.py:53
  223.4 3.0 %reduce_sum.45 = bf16[32,2,2048]{2,0,1:T(8,128)(2,1)S(1)} reduce(bf16[16,32,2,2048]{3,1,2,0:T(8,128)(2,1)} %all_to_all.34, bf16[]{:T(256)} %constant.43.clone.1), dimensions={0}, to_apply=%region_5.6 | reduce | flops 1966080 | bytes 4456450 | tf_op jit(solution)/shard_map/reduce_sum | solution.py:54
  226.4 1.0 copy.108
  227.4 14.3 %all-to-all-start.4 = ((bf16[32,2,2048]{2,1,0:T(2,128)(2,1)}), bf16[32,2,2048]{2,1,0:T(2,128)(2,1)S(1)}, u32[]{:S(2)}, u32[]{:S(2)}) async-start(bf16[32,2,2048]{2,1,0:T(2,128)(2,1)} %copy.108), calls=%async_computation.4 | async-start | bytes 524288 | tf_op jit(solution)/shard_map/all_to_all | solution.py:159
  241.7 22.2 %all-to-all-done.4 = bf16[32,2,2048]{2,1,0:T(2,128)(2,1)S(1)} async-done(((bf16[32,2,2048]{2,1,0:T(2,128)(2,1)}), bf16[32,2,2048]{2,1,0:T(2,128)(2,1)S(1)}, u32[]{:S(2)}, u32[]{:S(2)}) %all-to-all-start.4) | async-done | bytes 262176 | tf_op jit(solution)/shard_map/all_to_all | solution.py:159
  263.9 0.1 reshape.192
  264.0 0.2 convolution_multiply_fusion.1
  264.2 0.8 fusion.2
  (20 shorter events, 0.1 us)
Async XLA Ops:
  6.5 159.2 %copy-start = (bf16[1,320,2048]{2,1,0:T(8,128)(2,1)S(1)}, bf16[1,320,2048]{2,1,0:T(8,128)(2,1)}, u32[]{:S(2)}) copy-start(bf16[1,320,2048]{2,1,0:T(8,128)(2,1)} %param.23) | copy-start | bytes 3932164
  8.5 11.4 %collective-permute-start = (bf16[128,128]{1,0:T(8,128)(2,1)S(1)}, bf16[128,128]{1,0:T(8,128)(2,1)S(1)}, u32[]{:S(2)}, u32[]{:S(2)}) collective-permute-start(bf16[128,128]{1,0:T(8,128)(2,1)S(1)} %get-tuple-element.8), channel_id=1, source_target_pairs={{0,16},{16,32},{32,48},{48,64},{64,80},{80,96},{96,112},{112,128},... | collective-permute-start | bytes 98312 | tf_op jit(solution)/shard_map/ppermute | solution.py:21
  13.4 6.5 %collective-permute-start.1 = (bf16[128,128]{1,0:T(8,128)(2,1)S(1)}, bf16[128,128]{1,0:T(8,128)(2,1)S(1)}, u32[]{:S(2)}, u32[]{:S(2)}) collective-permute-start(bf16[128,128]{1,0:T(8,128)(2,1)S(1)} %get-tuple-element.9), channel_id=1, source_target_pairs={{16,0},{32,16},{48,32},{64,48},{80,64},{96,80},{112,96},{128,112},... | collective-permute-start | bytes 98312 | tf_op jit(solution)/shard_map/ppermute | solution.py:24
  18.9 1.8 copy-start.6
  22.5 5.7 %copy-start.5 = (s32[16,2]{0,1:T(2,128)S(1)}, s32[16,2]{0,1:T(2,128)}, u32[]{:S(2)}) copy-start(s32[16,2]{0,1:T(2,128)} %param.19) | copy-start | bytes 388
  22.5 22.2 %copy-start.3 = (bf16[2048,128]{1,0:T(8,128)(2,1)S(1)}, bf16[2048,128]{1,0:T(8,128)(2,1)}, u32[]{:S(2)}) copy-start(bf16[2048,128]{1,0:T(8,128)(2,1)} %param.16) | copy-start | bytes 1572868
  22.5 22.2 %all-to-all-start = ((bf16[16,256,128]{1,2,0:T(8,128)(2,1)}), bf16[16,256,128]{1,2,0:T(8,128)(2,1)S(1)}, u32[]{:S(2)}, u32[]{:S(2)}) async-start(bf16[16,256,128]{1,2,0:T(8,128)(2,1)} %broadcast_in_dim.16), calls=%async_computation | async-start | bytes 2097152 | tf_op jit(solution)/shard_map/all_to_all | solution.py:31
  28.2 28.0 %copy-start.2 = (bf16[16,2048]{1,0:T(8,128)(2,1)S(1)}, bf16[16,2048]{1,0:T(8,128)(2,1)}, u32[]{:S(2)}) copy-start(bf16[16,2048]{1,0:T(8,128)(2,1)} %param.17) | copy-start | bytes 196612
  28.2 28.1 %copy-start.4 = (f32[2048]{0:T(1024)S(1)}, f32[2048]{0:T(1024)}, u32[]{:S(2)}) copy-start(f32[2048]{0:T(1024)} %param.18) | copy-start | bytes 24580
  45.8 10.3 %all-to-all-start.1 = ((bf16[16,16,128]{2,1,0:T(8,128)(2,1)}), bf16[16,16,128]{2,1,0:T(8,128)(2,1)S(1)}, u32[]{:S(2)}, u32[]{:S(2)}) async-start(bf16[16,16,128]{2,1,0:T(8,128)(2,1)} %bitcast.14), calls=%async_computation.1 | async-start | bytes 131072 | tf_op jit(solution)/shard_map/all_to_all | solution.py:119
  49.3 102.7 %all-gather.2.cloned.1.call-start = ((), (), s32[]{:S(2)}) async-start(), calls=%async_computation.5 | async-start | bytes 4456448 | tf_op jit(solution)/shard_map/all_gather | solution.py:147
  97.6 61.6 %copy-start.8 = (bf16[1,2048,320]{1,2,0:T(8,128)(2,1)S(1)}, bf16[1,2048,320]{1,2,0:T(8,128)(2,1)}, u32[]{:S(2)}) copy-start(bf16[1,2048,320]{1,2,0:T(8,128)(2,1)} %param.21) | copy-start | bytes 3932164
  159.3 4.0 %copy-start.1 = (bf16[1024,2048]{1,0:T(8,128)(2,1)S(1)}, bf16[1024,2048]{1,0:T(8,128)(2,1)}, u32[]{:S(2)}) copy-start(bf16[1024,2048]{1,0:T(8,128)(2,1)} %reshape.190) | copy-start | bytes 12582916
  159.3 4.0 %copy-start.9 = (bf16[1,2048,320]{1,2,0:T(8,128)(2,1)S(1)}, bf16[1,2048,320]{1,2,0:T(8,128)(2,1)}, u32[]{:S(2)}) copy-start(bf16[1,2048,320]{1,2,0:T(8,128)(2,1)} %param.22) | copy-start | bytes 3932164
  223.4 18.2 %copy-start.7 = (f32[16,2]{0,1:T(2,128)S(1)}, f32[16,2]{0,1:T(2,128)}, u32[]{:S(2)}) copy-start(f32[16,2]{0,1:T(2,128)} %param.20) | copy-start | bytes 388
  227.4 36.5 %all-to-all-start.4 = ((bf16[32,2,2048]{2,1,0:T(2,128)(2,1)}), bf16[32,2,2048]{2,1,0:T(2,128)(2,1)S(1)}, u32[]{:S(2)}, u32[]{:S(2)}) async-start(bf16[32,2,2048]{2,1,0:T(2,128)(2,1)} %copy.108), calls=%async_computation.4 | async-start | bytes 524288 | tf_op jit(solution)/shard_map/all_to_all | solution.py:159
Sparse Core Ops, SparseCore 0:
  97.7 54.2 all-gather.1
where the time goes:
time: 273 us; the launch traced here: 272 us
  waiting for transfers between devices  99.2 us (36%)
  blocking collectives  95.6 us (35%)
  starting transfers between devices  33.5 us (12%)
  local copies, waits for them, and re-layouts  14.5 us (5%)
  between operations  13.8 us (5%)
  matrix products  10.9 us (4%)
  other arithmetic  4.35 us (2%)
    all_to_all x1, blocking collectives, summed_on_arrival(): lax.all_to_all(tiles, axis, split_axis=0, concat_axis=0, tiled=True)  54.8 us
    all_gather x1, waiting for transfers between devices, local(): lax.all_gather(lax.all_to_all(sending, 'sp', split_axis=0, concat_axis=0,...  54.4 us
    all_to_all x1, blocking collectives, local(): lax.all_to_all(sending, 'sp', split_axis=0, concat_axis=0, tiled=True)  40.8 us
    all_to_all x1, waiting for transfers between devices, local(): lax.all_to_all(summed_on_arrival(partial_value.astype(jnp.bfloat16), 'tp'...  22.2 us
    all_to_all x1, waiting for transfers between devices, sent_to_all(): return lax.all_to_all(copies, axis, split_axis=0, concat_axis=0, tiled=True)  15.9 us
    all_to_all x1, starting transfers between devices, local(): lax.all_to_all(summed_on_arrival(partial_value.astype(jnp.bfloat16), 'tp'...  14.3 us
    reshape x1, local copies, waits for them, and re-layouts, local(): flat = piece.reshape(-1, piece.shape[-1])  7.26 us
    all_to_all x1, waiting for transfers between devices, local(): lax.all_to_all(columns.astype(jnp.bfloat16), 'tp', split_axis=0, concat_a...  6.68 us
  transfers between devices with their start and end apart: 6, of which 4 were waited for; matrix products, arithmetic and copies ran while one was open for 1% of the time, Pallas kernels for 0%

commit v1 on v0

--- a/solution.py
+++ b/solution.py
@@ -1,6 +1,10 @@
+import functools
+
 import jax
 import jax.numpy as jnp
 from jax import lax
+from jax.experimental import pallas as pl
+from jax.experimental.pallas import tpu as pltpu
 from jax.sharding import PartitionSpec as P
 
 HEADS = 32
@@ -98,6 +102,324 @@
     return output.astype(jnp.bfloat16).reshape(length, groups * repeat * HEAD)
 
 
+UNITS = 4
+RING = 4
+MESH = pl.DeviceIdType.MESH
+
+
+def remote(src, dst, send_sem, recv_sem, device):
+    return pltpu.make_async_remote_copy(
+        src_ref=src, dst_ref=dst, send_sem=send_sem, recv_sem=recv_sem, device_id=device, device_id_type=MESH
+    )
+
+
+def moe_kernel(
+    count,
+    place_t_ref, first_ref, second_ref, rw_ref, normed_ref, hid_ref, wg_hbm, wu_hbm, wd_hbm,
+    out_ref,
+    wg, wu, wd, sending, arrived, x_all, p_all, half_s, full_s, sums, half_f, full_f, back_send, back,
+    w_sem, d_send, d_recv, b_send, b_recv, g_send, g_recv,
+):
+    me = lax.axis_index("sp")
+    tp = lax.axis_index("tp")
+    ty, tx = tp // RING, lax.rem(tp, RING)
+    rows = 2 * count // UNITS
+    per = count // UNITS
+
+    def shifted(pos, delta):
+        return lax.rem(pos + (delta + RING), RING)
+
+    def near(axis, delta):
+        if axis == "x":
+            return (me, ty * RING + shifted(tx, delta))
+        return (me, shifted(ty, delta) * RING + tx)
+
+    weight_copies = [
+        pltpu.make_async_copy(wg_hbm.at[0], wg, w_sem.at[0]),
+        pltpu.make_async_copy(wu_hbm.at[0], wu, w_sem.at[1]),
+        pltpu.make_async_copy(wd_hbm.at[0], wd, w_sem.at[2]),
+    ]
+    for copy in weight_copies:
+        copy.start()
+
+    barrier = pltpu.get_barrier_semaphore()
+
+    def greet(step, carry):
+        pl.semaphore_signal(barrier, inc=1, device_id=(lax.rem(me + step, count), tp), device_id_type=MESH)
+        return carry
+
+    lax.fori_loop(1, count, greet, 0)
+    for axis in ("x", "y"):
+        for delta in (1, -1):
+            pl.semaphore_signal(barrier, inc=1, device_id=near(axis, delta), device_id_type=MESH)
+
+    slots = jnp.dot(place_t_ref[...], normed_ref[...], preferred_element_type=jnp.float32).astype(jnp.bfloat16)
+    for expert in range(count):
+        sending[expert] = slots[2 * expert : 2 * expert + 2, :]
+    pl.semaphore_wait(barrier, count - 1 + 4)
+
+    def dispatch(step):
+        to = lax.rem(me + step, count)
+        return remote(
+            sending.at[to], arrived.at[count - step], d_send.at[step], d_recv.at[count - step], (to, tp)
+        )
+
+    def dispatch_pair(step, carry):
+        dispatch(step).start()
+        dispatch(count - step).start()
+        return carry
+
+    lax.fori_loop(1, count // 2, dispatch_pair, 0)
+    dispatch(count // 2).start()
+    arrived[0] = sending[me]
+
+    axes = [("x", "y"), ("x", "y"), ("y", "x"), ("y", "x")]
+    spot = {"x": tx, "y": ty}
+
+    def gcopy(unit, number, src, dst, axis, delta):
+        return remote(src, dst, g_send.at[unit, number], g_recv.at[unit, number], near(axis, delta))
+
+    started = []
+
+    def send(unit, number, src, dst, axis, delta):
+        copy = gcopy(unit, number, src, dst, axis, delta)
+        copy.start()
+        started.append(copy)
+
+    def landed(unit, number, dst):
+        gcopy(unit, number, dst, dst, "x", 1).wait_recv()
+
+    def g1(u):
+        first, second = axes[u]
+        f, s = spot[first], spot[second]
+        pieces = []
+        for j in range(per):
+            o = u * per + j
+            if o:
+                remote(arrived.at[o], arrived.at[o], d_send.at[o], d_recv.at[o], (me, tp)).wait_recv()
+            pieces.append(arrived[o])
+        for j in range(per):
+            x_all[u, s, f, 2 * j : 2 * j + 2, :] = pieces[j]
+        own = x_all.at[u, s, f]
+        send(u, 0, own, own, first, 1)
+        send(u, 1, own, own, first, -1)
+
+    def g2(u):
+        first, second = axes[u]
+        f, s = spot[first], spot[second]
+        h = rows // 2
+        low, high = x_all.at[u, s, shifted(f, -1)], x_all.at[u, s, shifted(f, 1)]
+        landed(u, 0, low)
+        send(u, 2, low.at[0:h], low.at[0:h], first, 1)
+        landed(u, 1, high)
+        send(u, 3, high.at[h:rows], high.at[h:rows], first, -1)
+
+    def g3(u):
+        first, second = axes[u]
+        f, s = spot[first], spot[second]
+        h = rows // 2
+        far = x_all.at[u, s, shifted(f, 2)]
+        landed(u, 2, far.at[0:h])
+        landed(u, 3, far.at[h:rows])
+        own = x_all.at[u, s]
+        send(u, 4, own, own, second, 1)
+        send(u, 5, own, own, second, -1)
+
+    def g4(u):
+        first, second = axes[u]
+        s = spot[second]
+        low, high = x_all.at[u, shifted(s, -1)], x_all.at[u, shifted(s, 1)]
+        landed(u, 4, low)
+        send(u, 6, low.at[0:2], low.at[0:2], second, 1)
+        landed(u, 5, high)
+        send(u, 7, high.at[2:4], high.at[2:4], second, -1)
+
+    def mlp(u):
+        first, second = axes[u]
+        s = spot[second]
+        far = x_all.at[u, shifted(s, 2)]
+        landed(u, 6, far.at[0:2])
+        landed(u, 7, far.at[2:4])
+        width = x_all.shape[-1]
+        flat = x_all[u].reshape(RING * RING * rows, width)
+        gate = jnp.dot(flat, wg[...], preferred_element_type=jnp.float32)
+        upward = jnp.dot(flat, wu[...], preferred_element_type=jnp.float32)
+        hidden = (gate / (1.0 + jnp.exp(-gate)) * upward).astype(jnp.bfloat16)
+        step = min(512, width)
+        for n in range(0, width, step):
+            part = jnp.dot(hidden, wd[:, n : n + step], preferred_element_type=jnp.float32)
+            p_all[u, :, :, :, n : n + step] = part.astype(jnp.bfloat16).reshape(RING, RING, rows, step)
+
+    def r1(u):
+        first, second = axes[u]
+        s = spot[second]
+        far = p_all.at[u, shifted(s, 2)]
+        send(u, 8, far.at[0:2], half_s.at[u, 0], second, 1)
+        send(u, 9, far.at[2:4], half_s.at[u, 1], second, -1)
+
+    def plus(a, b):
+        return (a.astype(jnp.float32) + b.astype(jnp.float32)).astype(jnp.bfloat16)
+
+    def r2(u):
+        first, second = axes[u]
+        s = spot[second]
+        up, down = shifted(s, 1), shifted(s, -1)
+        landed(u, 8, half_s.at[u, 0])
+        p_all[u, up, 0:2] = plus(p_all[u, up, 0:2], half_s[u, 0])
+        send(u, 10, p_all.at[u, up], full_s.at[u, 0], second, 1)
+        landed(u, 9, half_s.at[u, 1])
+        p_all[u, down, 2:4] = plus(p_all[u, down, 2:4], half_s[u, 1])
+        send(u, 11, p_all.at[u, down], full_s.at[u, 1], second, -1)
+
+    def r3(u):
+        first, second = axes[u]
+        f, s = spot[first], spot[second]
+        h = rows // 2
+        landed(u, 10, full_s.at[u, 0])
+        landed(u, 11, full_s.at[u, 1])
+        sums[u] = (
+            p_all[u, s].astype(jnp.float32)
+            + full_s[u, 0].astype(jnp.float32)
+            + full_s[u, 1].astype(jnp.float32)
+        ).astype(jnp.bfloat16)
+        far = sums.at[u, shifted(f, 2)]
+        send(u, 12, far.at[0:h], half_f.at[u, 0], first, 1)
+        send(u, 13, far.at[h:rows], half_f.at[u, 1], first, -1)
+
+    def r4(u):
+        first, second = axes[u]
+        f = spot[first]
+        h = rows // 2
+        up, down = shifted(f, 1), shifted(f, -1)
+        landed(u, 12, half_f.at[u, 0])
+        sums[u, up, 0:h] = plus(sums[u, up, 0:h], half_f[u, 0])
+        send(u, 14, sums.at[u, up], full_f.at[u, 0], first, 1)
+        landed(u, 13, half_f.at[u, 1])
+        sums[u, down, h:rows] = plus(sums[u, down, h:rows], half_f[u, 1])
+        send(u, 15, sums.at[u, down], full_f.at[u, 1], first, -1)
+
+    def giving_back(o):
+        to = lax.rem(me + o, count)
+        return remote(back_send.at[o], back.at[me], b_send.at[o], b_recv.at[me], (to, tp))
+
+    def r5(u):
+        first, second = axes[u]
+        f = spot[first]
+        landed(u, 14, full_f.at[u, 0])
+        landed(u, 15, full_f.at[u, 1])
+        total = (
+            sums[u, f].astype(jnp.float32)
+            + full_f[u, 0].astype(jnp.float32)
+            + full_f[u, 1].astype(jnp.float32)
+        ).astype(jnp.bfloat16)
+        for j in range(per):
+            o = u * per + j
+            if o:
+                back_send[o] = total[2 * j : 2 * j + 2, :]
+            else:
+                back[me] = total[0:2, :]
+        for j in range(per):
+            o = u * per + j
+            if o:
+                giving_back(o).start()
+
+    early, late = (0, 3), (1, 2)
+
+    def run(stage, pair):
+        for u in pair:
+            stage(u)
+
+    run(g1, early)
+    run(g2, early)
+    run(g1, late)
+    run(g3, early)
+    run(g2, late)
+    run(g4, early)
+    run(g3, late)
+    for copy in weight_copies:
+        copy.wait()
+    for u in early:
+        mlp(u)
+        r1(u)
+    run(g4, late)
+    run(r2, early)
+    for u in late:
+        mlp(u)
+        r1(u)
+    run(r3, early)
+    run(r2, late)
+    run(r4, early)
+    run(r3, late)
+    run(r5, early)
+    run(r4, late)
+    run(r5, late)
+
+    def came_back(step, carry):
+        sender = lax.rem(me + step, count)
+        remote(back.at[sender], back.at[sender], b_send.at[step], b_recv.at[sender], (me, tp)).wait_recv()
+        return carry
+
+    lax.fori_loop(1, count, came_back, 0)
+    table = jnp.concatenate([back[expert] for expert in range(count)], axis=0)
+    first_pick = jnp.dot(first_ref[...], table, preferred_element_type=jnp.float32)
+    second_pick = jnp.dot(second_ref[...], table, preferred_element_type=jnp.float32)
+    weights = rw_ref[...]
+    mixture = weights[:, 0:1] * first_pick + weights[:, 1:2] * second_pick
+    out_ref[...] = (hid_ref[...] + mixture).astype(jnp.bfloat16)
+
+    def sent(step, carry):
+        dispatch(step).wait_send()
+        giving_back(step).wait_send()
+        return carry
+
+    lax.fori_loop(1, count, sent, 0)
+    for copy in started:
+        copy.wait_send()
+
+
+def moe(place_t, first, second, route_weights, normed, hidden_state, gate_weight, up_weight, down_weight):
+    count = lax.axis_size("sp")
+    tokens, width = normed.shape
+    inner = gate_weight.shape[2]
+    rows = 2 * count // UNITS
+    bf16 = jnp.bfloat16
+    vmem = pl.BlockSpec(memory_space=pltpu.VMEM)
+    hbm = pl.BlockSpec(memory_space=pl.ANY)
+    return pl.pallas_call(
+        functools.partial(moe_kernel, count),
+        out_shape=jax.ShapeDtypeStruct((tokens, width), bf16),
+        in_specs=[vmem] * 6 + [hbm] * 3,
+        out_specs=vmem,
+        scratch_shapes=[
+            pltpu.VMEM((width, inner), bf16),
+            pltpu.VMEM((width, inner), bf16),
+            pltpu.VMEM((inner, width), bf16),
+            pltpu.VMEM((count, 2, width), bf16),
+            pltpu.VMEM((count, 2, width), bf16),
+            pltpu.VMEM((UNITS, RING, RING, rows, width), bf16),
+            pltpu.VMEM((UNITS, RING, RING, rows, width), bf16),
+            pltpu.VMEM((UNITS, 2, RING // 2, rows, width), bf16),
+            pltpu.VMEM((UNITS, 2, RING, rows, width), bf16),
+            pltpu.VMEM((UNITS, RING, rows, width), bf16),
+            pltpu.VMEM((UNITS, 2, rows // 2, width), bf16),
+            pltpu.VMEM((UNITS, 2, rows, width), bf16),
+            pltpu.VMEM((count, 2, width), bf16),
+            pltpu.VMEM((count, 2, width), bf16),
+            pltpu.SemaphoreType.DMA((3,)),
+            pltpu.SemaphoreType.DMA((count,)),
+            pltpu.SemaphoreType.DMA((count,)),
+            pltpu.SemaphoreType.DMA((count,)),
+            pltpu.SemaphoreType.DMA((count,)),
+            pltpu.SemaphoreType.DMA((UNITS, 16)),
+            pltpu.SemaphoreType.DMA((UNITS, 16)),
+        ],
+        compiler_params=pltpu.CompilerParams(
+            collective_id=0, has_side_effects=True, vmem_limit_bytes=60 * 1024 * 1024
+        ),
+        name="moe",
+    )(place_t, first, second, route_weights, normed, hidden_state, gate_weight, up_weight, down_weight)
+
+
 def local(
     queries,
     keys,
@@ -124,7 +446,6 @@
     normed = (hidden_state * inverse * norm_gain).astype(jnp.bfloat16)
     sp_count = lax.axis_size("sp")
     tok_rows = residual.shape[0]
-    width = residual.shape[1]
     capacity = max(2, 4 * tok_rows // sp_count)
     slot_total = sp_count * capacity
     expert_ids = routes.reshape(-1)
@@ -134,40 +455,17 @@
     earlier = jnp.cumsum(onehot, axis=0) - onehot
     rank = jnp.sum(earlier * onehot, axis=1)
     slots = expert_ids * capacity + rank
-    placing = (slots[:, None] == jnp.arange(slot_total, dtype=jnp.int32)[None, :]).astype(
-        jnp.bfloat16
-    )
-    placing = placing.reshape(tok_rows, 2, slot_total)
-    first_place = placing[:, 0]
-    second_place = placing[:, 1]
-    sending = jnp.einsum(
-        "ts,td->sd", first_place + second_place, normed, preferred_element_type=jnp.float32
-    )
-    sending = sending.astype(jnp.bfloat16).reshape(sp_count, capacity, width)
-    piece = lax.all_gather(
-        lax.all_to_all(sending, "sp", split_axis=0, concat_axis=0, tiled=True),
-        "tp",
-        axis=0,
-        tiled=True,
-    )
-    flat = piece.reshape(-1, piece.shape[-1])
-    gate = jnp.dot(flat, gate_weight[0], preferred_element_type=jnp.float32)
-    upward = jnp.dot(flat, up_weight[0], preferred_element_type=jnp.float32)
-    hidden = (jax.nn.silu(gate) * upward).astype(jnp.bfloat16)
-    partial_value = jnp.dot(hidden, down_weight[0], preferred_element_type=jnp.float32)
-    partial_value = partial_value.reshape(piece.shape[:-1] + (down_weight.shape[-1],))
-    returned = lax.all_to_all(
-        summed_on_arrival(partial_value.astype(jnp.bfloat16), "tp", 0).astype(jnp.bfloat16),
-        "sp",
-        split_axis=0,
-        concat_axis=0,
-        tiled=True,
-    )
-    gathered_back = returned.reshape(slot_total, width)
-    first_pick = jnp.dot(first_place, gathered_back, preferred_element_type=jnp.float32)
-    second_pick = jnp.dot(second_place, gathered_back, preferred_element_type=jnp.float32)
-    mixture = route_weights[:, 0:1] * first_pick + route_weights[:, 1:2] * second_pick
-    return (hidden_state + mixture).astype(jnp.bfloat16)
+    slot_ids = jnp.arange(slot_total, dtype=jnp.int32)
+    pairs = slots.reshape(tok_rows, 2)
+    first_place = (pairs[:, 0:1] == slot_ids[None, :]).astype(jnp.bfloat16)
+    second_place = (pairs[:, 1:2] == slot_ids[None, :]).astype(jnp.bfloat16)
+    place_t = (
+        (pairs[:, 0][None, :] == slot_ids[:, None]) | (pairs[:, 1][None, :] == slot_ids[:, None])
+    ).astype(jnp.bfloat16)
+    return moe(
+        place_t, first_place, second_place, route_weights, normed, hidden_state,
+        gate_weight, up_weight, down_weight,
+    )
 
 
 def solution(mesh):

time: 273 us -> 147 us (0.54)
  blocking collectives: 95.6 us -> 0 us
  Pallas kernels: 0 us -> 94.7 us
  waiting for transfers between devices: 99.2 us -> 17.4 us
  starting transfers between devices: 33.5 us -> 18.5 us
  between operations: 13.8 us -> 0.25 us
  matrix products: 10.9 us -> 1.7 us
  local copies, waits for them, and re-layouts: 14.5 us -> 10.6 us
    all_to_all x2 -> x0, blocking collectives: 95.6 us -> none  [the longest x1 54.8 us: summed_on_arrival(): lax.all_to_all(tiles, axis, split_axis=0, concat_axis=0, tiled=True)]
    pallas_call x0 -> x1, Pallas kernels: none -> 94.7 us  [moe(): pl.pallas_call(functools.partial(moe_kernel, count), out_shape=jax.ShapeD...]
    all_gather x1 -> x0, waiting for transfers between devices: 54.4 us -> none  [local(): lax.all_gather(lax.all_to_all(sending, 'sp', split_axis=0, concat_axis=0,...]
    all_to_all x1 -> x0, waiting for transfers between devices: 22.2 us -> none  [local(): lax.all_to_all(summed_on_arrival(partial_value.astype(jnp.bfloat16), 'tp'...]
    all_to_all x1 -> x0, starting transfers between devices: 14.3 us -> none  [local(): lax.all_to_all(summed_on_arrival(partial_value.astype(jnp.bfloat16), 'tp'...]
    dot_general x6 -> x0, matrix products: 9.25 us -> none  [the longest x1 4 us: local(): gate = jnp.dot(flat, gate_weight[0], preferred_element_type=jnp.float32)]
    reshape x4 -> x0, local copies, waits for them, and re-layouts: 8.12 us -> none  [the longest x1 7.26 us: local(): flat = piece.reshape(-1, piece.shape[-1])]
    unnamed x24 -> x26, local copies, waits for them, and re-layouts: 1.99 us -> 7.88 us
  transfers between devices with their start and end apart: 6 -> 4, of which waited for: 4 -> 2; matrix products, arithmetic and copies ran while one was open for 1% -> 5% of each run, Pallas kernels for 0% -> 0%
where the time goes in v1:
time: 147 us; the launch traced here: 146 us
  Pallas kernels  94.7 us (64%)
  starting transfers between devices  18.5 us (13%)
  waiting for transfers between devices  17.4 us (12%)
  local copies, waits for them, and re-layouts  10.6 us (7%)
  other arithmetic  3.29 us (2%)
  matrix products  1.7 us (1%)
    pallas_call x1, Pallas kernels, moe(): pl.pallas_call(functools.partial(moe_kernel, count), out_shape=jax.ShapeD...  94.7 us
    all_to_all x1, waiting for transfers between devices, sent_to_all(): return lax.all_to_all(copies, axis, split_axis=0, concat_axis=0, tiled=True)  15.5 us
    unnamed x26, local copies, waits for them, and re-layouts  7.88 us
    ppermute x1, starting transfers between devices, with_halo(): lax.ppermute(lax.slice_in_dim(block, 0, width, axis=dim), axis, backward)  5.11 us
    ppermute x1, starting transfers between devices, with_halo(): lax.ppermute(lax.slice_in_dim(block, block.shape[dim] - width, None, axis...  4.92 us
    all_to_all x1, starting transfers between devices, sent_to_all(): return lax.all_to_all(copies, axis, split_axis=0, concat_axis=0, tiled=True)  4.81 us
    all_to_all x1, starting transfers between devices, local(): lax.all_to_all(columns.astype(jnp.bfloat16), 'tp', split_axis=0, concat_a...  3.68 us
  transfers between devices with their start and end apart: 4, of which 2 were waited for; matrix products, arithmetic and copies ran while one was open for 5% of the time, Pallas kernels for 0%

profile of v1, /device:TPU:1, one launch (start us, length us, event | category | flops | bytes accessed | tf_op | source)
XLA Modules:
  0.0 146.4 jit_solution(12270586944672510763)
XLA Ops:
  0.0 0.0 copy-start
  0.0 0.9 copy.56
  0.9 0.9 copy.57
  1.8 0.1 fusion.6
  1.9 4.9 %collective-permute-start = (bf16[128,128]{1,0:T(8,128)(2,1)S(1)}, bf16[128,128]{1,0:T(8,128)(2,1)S(1)}, u32[]{:S(2)}, u32[]{:S(2)}) collective-permute-start(bf16[128,128]{1,0:T(8,128)(2,1)S(1)} %get-tuple-element.10), channel_id=1, source_target_pairs={{0,16},{16,32},{32,48},{48,64},{64,80},{80,96},{96,112},{112,128},... | collective-permute-start | bytes 98312 | tf_op jit(solution)/shard_map/ppermute | solution.py:25
  6.8 5.1 %collective-permute-start.1 = (bf16[128,128]{1,0:T(8,128)(2,1)S(1)}, bf16[128,128]{1,0:T(8,128)(2,1)S(1)}, u32[]{:S(2)}, u32[]{:S(2)}) collective-permute-start(bf16[128,128]{1,0:T(8,128)(2,1)S(1)} %get-tuple-element.11), channel_id=1, source_target_pairs={{16,0},{32,16},{48,32},{64,48},{80,64},{96,80},{112,96},{128,112},... | collective-permute-start | bytes 98312 | tf_op jit(solution)/shard_map/ppermute | solution.py:28
  12.0 0.1 compare_and_fusion
  12.1 0.1 abs_compare_fusion
  12.1 0.2 broadcast_and_fusion
  12.3 0.0 copy-start.7
  12.3 0.8 copy.54
  13.1 0.1 eq.71
  13.2 0.9 reshape.156
  14.1 0.0 collective-permute-done
  14.1 0.0 collective-permute-done.1
  14.2 0.1 pad_maximum_fusion.3
  14.3 0.1 copy.58
  14.4 0.1 copy.60
  14.5 0.1 copy.59
  14.7 0.3 fusion.13
  15.0 0.0 copy-done.7
  15.0 0.1 broadcast_maximum_fusion
  15.1 0.1 fusion.3
  15.2 0.1 exponential_add_fusion
  15.3 0.3 fusion.2
  15.6 0.1 copy.64
  15.7 1.1 broadcast_in_dim.16
  16.8 0.0 copy-start.6
  16.8 4.8 %all-to-all-start = ((bf16[16,256,128]{1,2,0:T(8,128)(2,1)}), bf16[16,256,128]{1,2,0:T(8,128)(2,1)S(1)}, u32[]{:S(2)}, u32[]{:S(2)}) async-start(bf16[16,256,128]{1,2,0:T(8,128)(2,1)} %broadcast_in_dim.16), calls=%async_computation | async-start | bytes 2097152 | tf_op jit(solution)/shard_map/all_to_all | solution.py:35
  21.6 0.0 copy-start.8
  21.6 0.0 copy-start.1
  21.6 0.1 fusion.10
  21.7 0.1 reduce_window_sum.11
  21.7 0.2 select_reduce_fusion
  21.9 0.1 reduce_sum.30
  22.0 0.1 copy.55
  22.1 0.0 copy-done.6
  22.1 0.6 fusion.9.place_t_ref
  22.7 15.5 %all-to-all-done = bf16[16,256,128]{1,2,0:T(8,128)(2,1)S(1)} async-done(((bf16[16,256,128]{1,2,0:T(8,128)(2,1)}), bf16[16,256,128]{1,2,0:T(8,128)(2,1)S(1)}, u32[]{:S(2)}, u32[]{:S(2)}) %all-to-all-start) | async-done | bytes 1048608 | tf_op jit(solution)/shard_map/all_to_all | solution.py:35
  38.2 0.0 copy-done
  38.2 1.1 convolution_convert_fusion
  39.3 3.7 %all-to-all-start.1 = ((bf16[16,16,128]{2,1,0:T(8,128)(2,1)}), bf16[16,16,128]{2,1,0:T(8,128)(2,1)S(1)}, u32[]{:S(2)}, u32[]{:S(2)}) async-start(bf16[16,16,128]{2,1,0:T(8,128)(2,1)} %bitcast.16), calls=%async_computation.1 | async-start | bytes 131072 | tf_op jit(solution)/shard_map/all_to_all | solution.py:441
  43.0 0.7 fusion.11
  43.7 0.0 copy-done.8
  43.7 0.7 copy.66.rw_ref
  44.4 0.0 copy-done.1
  44.4 0.0 copy-start.2
  44.4 1.6 %copy.67.wg_hbm = bf16[1,2048,320]{2,1,0:T(8,128)(2,1)} copy(bf16[1,2048,320]{1,2,0:T(8,128)(2,1)S(1)} %copy-done.1) | data formatting | bytes 2621440 | tf_op args[9]
  45.9 0.0 copy-done.2
  45.9 0.0 copy-start.4
  45.9 0.0 copy-start.5
  45.9 1.6 %copy.68.wu_hbm = bf16[1,2048,320]{2,1,0:T(8,128)(2,1)} copy(bf16[1,2048,320]{1,2,0:T(8,128)(2,1)S(1)} %copy-done.2) | data formatting | bytes 2621440 | tf_op args[10]
  47.5 1.9 %all-to-all-done.1 = bf16[16,16,128]{2,1,0:T(8,128)(2,1)S(1)} async-done(((bf16[16,16,128]{2,1,0:T(8,128)(2,1)}), bf16[16,16,128]{2,1,0:T(8,128)(2,1)S(1)}, u32[]{:S(2)}, u32[]{:S(2)}) %all-to-all-start.1) | async-done | bytes 65568 | tf_op jit(solution)/shard_map/all_to_all | solution.py:441
  49.4 0.0 copy-done.4
  49.4 0.1 multiply_reduce_fusion
  49.5 0.0 copy-start.3
  49.6 0.0 copy-done.5
  49.6 0.7 multiply_convert_fusion.normed_ref
  50.3 0.0 copy-done.3
  50.3 94.7 %moe.1 = bf16[16,2048]{1,0:T(8,128)(2,1)} custom-call(bf16[64,16]{1,0:T(8,128)(2,1)} %fusion.9.place_t_ref, bf16[16,64]{1,0:T(8,128)(2,1)} %get-tuple-element.16.first_ref, bf16[16,64]{1,0:T(8,128)(2,1)} %get-tuple-element.17.second_ref, f32[16,2]{1,0:T(8,128)} %copy.66.rw_ref, bf16[16,2048]{1,0:T(8,128)(2,1)} %multiply_convert_fusion.normed_ref, ...), custom_call_target="tpu_custom_call" | custom-call | tf_op jit(solution)/shard_map/moe/pallas_call | solution.py:388
  145.0 1.5 %copy.85 = bf16[16,2048]{1,0:T(8,128)(2,1)} copy(bf16[16,2048]{1,0:T(8,128)(2,1)} %moe.1) | data formatting | bytes 131072
  (7 shorter events, 0.1 us)
Async XLA Ops:
  0.0 38.2 %copy-start = (bf16[2048,128]{1,0:T(8,128)(2,1)S(1)}, bf16[2048,128]{1,0:T(8,128)(2,1)}, u32[]{:S(2)}) copy-start(bf16[2048,128]{1,0:T(8,128)(2,1)} %param.16) | copy-start | bytes 1572868
  1.9 12.2 %collective-permute-start = (bf16[128,128]{1,0:T(8,128)(2,1)S(1)}, bf16[128,128]{1,0:T(8,128)(2,1)S(1)}, u32[]{:S(2)}, u32[]{:S(2)}) collective-permute-start(bf16[128,128]{1,0:T(8,128)(2,1)S(1)} %get-tuple-element.10), channel_id=1, source_target_pairs={{0,16},{16,32},{32,48},{48,64},{64,80},{80,96},{96,112},{112,128},... | collective-permute-start | bytes 98312 | tf_op jit(solution)/shard_map/ppermute | solution.py:25
  6.8 7.3 %collective-permute-start.1 = (bf16[128,128]{1,0:T(8,128)(2,1)S(1)}, bf16[128,128]{1,0:T(8,128)(2,1)S(1)}, u32[]{:S(2)}, u32[]{:S(2)}) collective-permute-start(bf16[128,128]{1,0:T(8,128)(2,1)S(1)} %get-tuple-element.11), channel_id=1, source_target_pairs={{16,0},{32,16},{48,32},{64,48},{80,64},{96,80},{112,96},{128,112},... | collective-permute-start | bytes 98312 | tf_op jit(solution)/shard_map/ppermute | solution.py:28
  12.3 2.7 %copy-start.7 = (f32[2]{0:T(128)S(1)}, f32[2]{0:T(128)}, u32[]{:S(2)}) copy-start(f32[2]{0:T(128)} %param.15) | copy-start | bytes 28
  16.8 5.3 %copy-start.6 = (s32[16,2]{0,1:T(2,128)S(1)}, s32[16,2]{0,1:T(2,128)}, u32[]{:S(2)}) copy-start(s32[16,2]{0,1:T(2,128)} %param.19) | copy-start | bytes 388
  16.8 21.5 %all-to-all-start = ((bf16[16,256,128]{1,2,0:T(8,128)(2,1)}), bf16[16,256,128]{1,2,0:T(8,128)(2,1)S(1)}, u32[]{:S(2)}, u32[]{:S(2)}) async-start(bf16[16,256,128]{1,2,0:T(8,128)(2,1)} %broadcast_in_dim.16), calls=%async_computation | async-start | bytes 2097152 | tf_op jit(solution)/shard_map/all_to_all | solution.py:35
  21.6 22.1 %copy-start.8 = (f32[16,2]{0,1:T(2,128)S(1)}, f32[16,2]{0,1:T(2,128)}, u32[]{:S(2)}) copy-start(f32[16,2]{0,1:T(2,128)} %param.20) | copy-start | bytes 388
  21.6 22.8 %copy-start.1 = (bf16[1,2048,320]{1,2,0:T(8,128)(2,1)S(1)}, bf16[1,2048,320]{1,2,0:T(8,128)(2,1)}, u32[]{:S(2)}) copy-start(bf16[1,2048,320]{1,2,0:T(8,128)(2,1)} %param.21) | copy-start | bytes 3932164
  39.3 10.1 %all-to-all-start.1 = ((bf16[16,16,128]{2,1,0:T(8,128)(2,1)}), bf16[16,16,128]{2,1,0:T(8,128)(2,1)S(1)}, u32[]{:S(2)}, u32[]{:S(2)}) async-start(bf16[16,16,128]{2,1,0:T(8,128)(2,1)} %bitcast.16), calls=%async_computation.1 | async-start | bytes 131072 | tf_op jit(solution)/shard_map/all_to_all | solution.py:441
  44.4 1.6 %copy-start.2 = (bf16[1,2048,320]{1,2,0:T(8,128)(2,1)S(1)}, bf16[1,2048,320]{1,2,0:T(8,128)(2,1)}, u32[]{:S(2)}) copy-start(bf16[1,2048,320]{1,2,0:T(8,128)(2,1)} %param.22) | copy-start | bytes 3932164
  45.9 3.5 %copy-start.4 = (bf16[16,2048]{1,0:T(8,128)(2,1)S(1)}, bf16[16,2048]{1,0:T(8,128)(2,1)}, u32[]{:S(2)}) copy-start(bf16[16,2048]{1,0:T(8,128)(2,1)} %param.17) | copy-start | bytes 196612
  45.9 3.6 %copy-start.5 = (f32[2048]{0:T(1024)S(1)}, f32[2048]{0:T(1024)}, u32[]{:S(2)}) copy-start(f32[2048]{0:T(1024)} %param.18) | copy-start | bytes 24580
  49.5 0.7 copy-start.3

commit v2 on v0

v2 whole, which is shorter than its diff:
```python
import functools

import jax
import jax.numpy as jnp
from jax import lax
from jax.experimental import pallas as pl
from jax.experimental.pallas import tpu as pltpu
from jax.sharding import PartitionSpec as P

HEADS = 32
KV_HEADS = 16
HEAD = 64
WINDOW = 128
EPS = 1e-06
NEGATIVE = -1e30

UNITS = 4
RING = 4
MESH = pl.DeviceIdType.MESH
BF16 = jnp.bfloat16
F32 = jnp.float32


def remote(src, dst, send_sem, recv_sem, device):
    return pltpu.make_async_remote_copy(
        src_ref=src, dst_ref=dst, send_sem=send_sem, recv_sem=recv_sem, device_id=device, device_id_type=MESH
    )


def contract_last(a, b):
    return lax.dot_general(a, b, (((1,), (1,)), ((), ())), preferred_element_type=F32)


def kernel(
    count,
    q_ref, kt_ref, vt_ref, sink_ref, w_ref, res_ref, gain_ref, routes_ref, rw_ref, wg_hbm, wu_hbm, wd_hbm,
    out_ref,
    wg, wu, wd, k_ext, v_ext, w_rows, attn, hid,
    sending, arrived, x_all, p_all, half_s, full_s, sums, half_f, full_f,
    pp_all, phalf_s, pfull_s, psums, phalf_f, pfull_f,
    back_send, back,
    w_sem, h_send, h_recv, o_send, o_recv, d_send, d_recv, b_send, b_recv, g_send, g_recv, r_send, r_recv, p_send, p_recv,
):
    me = lax.axis_index("sp")
    tp = lax.axis_index("tp")
    peers = RING * RING
    ty, tx = tp // RING, lax.rem(tp, RING)
    spot = {"x": tx, "y": ty}
    rows = 2 * count // UNITS
    per = count // UNITS
    tokens, width = hid.shape
    length = q_ref.shape[0]
    groups = length // WINDOW

    def shifted(pos, delta):
        return lax.rem(pos + (delta + RING), RING)

    def near(axis, delta):
        if axis == "x":
            return (me, ty * RING + shifted(tx, delta))
        return (me, shifted(ty, delta) * RING + tx)

    weight_copies = [
        pltpu.make_async_copy(wg_hbm.at[0], wg, w_sem.at[0]),
        pltpu.make_async_copy(wu_hbm.at[0], wu, w_sem.at[1]),
        pltpu.make_async_copy(wd_hbm.at[0], wd, w_sem.at[2]),
    ]
    for copy in weight_copies:
        copy.start()

    barrier = pltpu.get_barrier_semaphore()

    def greet_sp(step, carry):
        pl.semaphore_signal(barrier, inc=1, device_id=(lax.rem(me + step, count), tp), device_id_type=MESH)
        return carry

    def greet_tp(step, carry):
        pl.semaphore_signal(barrier, inc=1, device_id=(me, lax.rem(tp + step, peers)), device_id_type=MESH)
        return carry

    lax.fori_loop(1, count, greet_sp, 0)
    lax.fori_loop(1, peers, greet_tp, 0)

    t_row = lax.broadcasted_iota(jnp.int32, (tokens, tokens), 0)
    t_col = lax.broadcasted_iota(jnp.int32, (tokens, tokens), 1)

    def as_column(row):
        spread = jnp.where(t_row == t_col, jnp.broadcast_to(row, (tokens, tokens)), 0.0)
        return jnp.sum(spread, axis=1, keepdims=True)

    named = [routes_ref[a : a + 1, :].astype(F32) for a in range(2)]
    named_column = [as_column(row) for row in named]
    slot = []
    for row in named:
        rank = jnp.zeros((1, tokens), F32)
        for column in named_column:
            same = (column == row) & (t_row < t_col)
            rank = rank + jnp.sum(jnp.where(same, 1.0, 0.0), axis=0, keepdims=True)
        slot.append(2.0 * row + rank)
    slot_down = lax.broadcasted_iota(jnp.int32, (2 * count, tokens), 0).astype(F32)
    slot_across = lax.broadcasted_iota(jnp.int32, (tokens, 2 * count), 1).astype(F32)
    placed = jnp.where((slot_down == slot[0]) | (slot_down == slot[1]), 1.0, 0.0).astype(BF16)
    picks = [jnp.where(slot_across == as_column(row), 1.0, 0.0).astype(BF16) for row in slot]
    route_weight = [as_column(rw_ref[a : a + 1, :]) for a in range(2)]

    k_ext[:, WINDOW : WINDOW + length] = kt_ref[...]
    v_ext[:, WINDOW : WINDOW + length] = vt_ref[...]
    block = pl.ds(pl.multiple_of(tp * WINDOW, WINDOW), WINDOW)
    w_rows[:, block] = w_ref[block, :]

    pl.semaphore_wait(barrier, count - 1 + peers - 1)

    right, left = lax.rem(me + 1, count), lax.rem(me + count - 1, count)
    halo = []
    for i, (own, ext) in enumerate(((kt_ref, k_ext), (vt_ref, v_ext))):
        halo.append(
            remote(
                own.at[:, length - WINDOW : length], ext.at[:, 0:WINDOW], h_send.at[2 * i], h_recv.at[2 * i], (right, tp)
            )
        )
        halo.append(
            remote(
                own.at[:, 0:WINDOW], ext.at[:, WINDOW + length : 2 * WINDOW + length],
                h_send.at[2 * i + 1], h_recv.at[2 * i + 1], (left, tp),
            )
        )
    for copy in halo:
        copy.start()

    def columns_to(step):
        to = lax.rem(tp + step, peers)
        return remote(
            w_ref.at[pl.ds(pl.multiple_of(to * WINDOW, WINDOW), WINDOW), :],
            w_rows.at[:, block],
            o_send.at[step], o_recv.at[step], (me, to),
        )

    def send_columns(step, carry):
        columns_to(step).start()
        return carry

    lax.fori_loop(1, peers, send_columns, 0)

    for copy in halo:
        copy.wait_recv()
    row_i = lax.broadcasted_iota(jnp.int32, (WINDOW, 3 * WINDOW), 0)
    col_j = lax.broadcasted_iota(jnp.int32, (WINDOW, 3 * WINDOW), 1)
    close = (col_j >= row_i) & (col_j <= row_i + 2 * WINDOW)
    for n in range(groups):
        position = me * length + (n - 1) * WINDOW + col_j
        valid = close & (position >= 0) & (position < length * count)
        band = slice(n * WINDOW, (n + 3) * WINDOW)
        for r in range(HEADS // KV_HEADS):
            query = q_ref[n * WINDOW : (n + 1) * WINDOW, r * HEAD : (r + 1) * HEAD]
            scores = jnp.dot(query, k_ext[:, band], preferred_element_type=F32) * HEAD ** (-0.5)
            sink = jnp.full((WINDOW, 1), sink_ref[r], F32)
            masked = jnp.where(valid, scores, NEGATIVE)
            top = jnp.maximum(jnp.max(masked, axis=-1, keepdims=True), sink)
            probs = jnp.exp(masked - top)
            denom = jnp.sum(probs, axis=-1, keepdims=True) + jnp.exp(sink - top)
            weights = (probs / denom).astype(BF16)
            attn[n * WINDOW : (n + 1) * WINDOW, r * HEAD : (r + 1) * HEAD] = contract_last(
                weights, v_ext[:, band]
            ).astype(BF16)

    def columns_here(step, carry):
        source = lax.rem(tp + (peers - step), peers)
        place = w_rows.at[:, pl.ds(pl.multiple_of(source * WINDOW, WINDOW), WINDOW)]
        remote(place, place, o_send.at[step], o_recv.at[step], (me, tp)).wait_recv()
        return carry

    lax.fori_loop(1, peers, columns_here, 0)

    started = []

    class Reduction:
        def __init__(self, axes, parts, hs, fs, total, hf, ff, send_sem, recv_sem):
            self.first, self.second = axes
            self.f, self.s = spot[self.first], spot[self.second]
            self.parts, self.hs, self.fs, self.total, self.hf, self.ff = parts, hs, fs, total, hf, ff
            self.send_sem, self.recv_sem = send_sem, recv_sem
            self.rows = parts.shape[2]
            self.half = self.rows // 2

        def copy(self, number, src, dst, axis, delta):
            return remote(src, dst, self.send_sem.at[number], self.recv_sem.at[number], near(axis, delta))

        def send(self, number, src, dst, axis, delta):
            copy = self.copy(number, src, dst, axis, delta)
            copy.start()
            started.append(copy)

        def landed(self, number, dst):
            self.copy(number, dst, dst, "x", 1).wait_recv()

        def at(self, k):
            return shifted(self.f, (0, -1, 1, 2)[k])

        def begin(self):
            h, far = self.half, shifted(self.s, 2)
            for k in (3, 1, 2, 0):
                src = self.parts.at[far, self.at(k)]
                self.send(2 * k, src.at[0:h], self.hs.at[0, k], self.second, 1)
                self.send(2 * k + 1, src.at[h : 2 * h], self.hs.at[1, k], self.second, -1)

        def relay(self, k):
            h, fk = self.half, self.at(k)
            up, down = shifted(self.s, 1), shifted(self.s, -1)
            self.landed(2 * k, self.hs.at[0, k])
            self.parts[up, fk, 0:h] = (self.parts[up, fk, 0:h].astype(F32) + self.hs[0, k].astype(F32)).astype(BF16)
            self.send(8 + 2 * k, self.parts.at[up, fk], self.fs.at[0, k], self.second, 1)
            self.landed(2 * k + 1, self.hs.at[1, k])
            self.parts[down, fk, h : 2 * h] = (
                self.parts[down, fk, h : 2 * h].astype(F32) + self.hs[1, k].astype(F32)
            ).astype(BF16)
            self.send(9 + 2 * k, self.parts.at[down, fk], self.fs.at[1, k], self.second, -1)

        def summed(self, k):
            self.landed(8 + 2 * k, self.fs.at[0, k])
            self.landed(9 + 2 * k, self.fs.at[1, k])
            return self.parts[self.s, self.at(k)].astype(F32) + self.fs[0, k].astype(F32) + self.fs[1, k].astype(F32)

        def turn(self):
            h = self.half
            self.total[3] = self.summed(3).astype(BF16)
            self.send(16, self.total.at[3, 0:h], self.hf.at[0], self.first, 1)
            self.send(17, self.total.at[3, h : 2 * h], self.hf.at[1], self.first, -1)

        def cross(self):
            h = self.half
            high = self.summed(2)
            self.landed(16, self.hf.at[0])
            self.total[2, 0:h] = (high[0:h] + self.hf[0].astype(F32)).astype(BF16)
            self.total[2, h : 2 * h] = high[h:].astype(BF16)
            self.send(18, self.total.at[2], self.ff.at[0], self.first, 1)
            low = self.summed(1)
            self.landed(17, self.hf.at[1])
            self.total[1, 0:h] = low[0:h].astype(BF16)
            self.total[1, h : 2 * h] = (low[h:] + self.hf[1].astype(F32)).astype(BF16)
            self.send(19, self.total.at[1], self.ff.at[1], self.first, -1)

        def finish(self):
            own = self.summed(0)
            self.landed(18, self.ff.at[0])
            self.landed(19, self.ff.at[1])
            return own + self.ff[0].astype(F32) + self.ff[1].astype(F32)

    part_width = width // 2
    step_width = min(512, part_width)
    for n in range(0, width, step_width):
        part = jnp.dot(attn[...], w_rows[:, n : n + step_width], preferred_element_type=F32).astype(BF16)
        color, at = n // part_width, n % part_width
        for t in range(peers):
            y, x = t // RING, t % RING
            i, j = (y, x) if color == 0 else (x, y)
            pp_all[color, i, j, :, at : at + step_width] = part[t * tokens : (t + 1) * tokens, :]

    projections = [
        Reduction(
            (("x", "y"), ("y", "x"))[c], pp_all.at[c], phalf_s.at[c], pfull_s.at[c], psums.at[c], phalf_f.at[c],
            pfull_f.at[c], p_send.at[c], p_recv.at[c],
        )
        for c in range(2)
    ]
    for red in projections:
        red.begin()
    for k in (3, 1, 2, 0):
        for red in projections:
            red.relay(k)
    for red in projections:
        red.turn()
    for red in projections:
        red.cross()
    for c, red in enumerate(projections):
        columns = slice(c * part_width, (c + 1) * part_width)
        hid[:, columns] = res_ref[:, columns].astype(F32) + red.finish()

    hidden_state = hid[...]
    inverse = lax.rsqrt(jnp.mean(hidden_state * hidden_state, axis=-1, keepdims=True) + EPS)
    normed = (hidden_state * inverse * gain_ref[...]).astype(BF16)
    slots = jnp.dot(placed, normed, preferred_element_type=F32).astype(BF16)
    for expert in range(count):
        sending[expert] = slots[2 * expert : 2 * expert + 2, :]

    def dispatch(step):
        to = lax.rem(me + step, count)
        return remote(
            sending.at[to], arrived.at[count - step], d_send.at[step], d_recv.at[count - step], (to, tp)
        )

    def dispatch_pair(step, carry):
        dispatch(step).start()
        dispatch(count - step).start()
        return carry

    lax.fori_loop(1, count // 2, dispatch_pair, 0)
    dispatch(count // 2).start()
    arrived[0] = sending[me]

    class Gather:
        def __init__(self, unit, axes):
            self.unit = unit
            self.first, self.second = axes
            self.f, self.s = spot[self.first], spot[self.second]
            self.x = x_all.at[unit]
            self.half = rows // 2

        def copy(self, number, src, dst, axis, delta):
            return remote(src, dst, g_send.at[self.unit, number], g_recv.at[self.unit, number], near(axis, delta))

        def send(self, number, ref, axis, delta):
            copy = self.copy(number, ref, ref, axis, delta)
            copy.start()
            started.append(copy)

        def landed(self, number, dst):
            self.copy(number, dst, dst, "x", 1).wait_recv()

        def at(self, k):
            return shifted(self.f, (0, -1, 1, 2)[k])

        def across(self, k):
            own = self.x.at[self.s, self.at(k)]
            self.send(4 + 2 * k, own, self.second, 1)
            self.send(5 + 2 * k, own, self.second, -1)

        def begin(self):
            pieces = []
            for j in range(per):
                o = self.unit * per + j
                if o:
                    remote(arrived.at[o], arrived.at[o], d_send.at[o], d_recv.at[o], (me, tp)).wait_recv()
                pieces.append(arrived[o])
            for j in range(per):
                self.x[self.s, self.f, 2 * j : 2 * j + 2, :] = pieces[j]
            own = self.x.at[self.s, self.f]
            self.send(0, own, self.first, 1)
            self.send(1, own, self.first, -1)
            self.across(0)

        def along(self):
            h = self.half
            low, high = self.x.at[self.s, self.at(1)], self.x.at[self.s, self.at(2)]
            self.landed(0, low)
            self.send(2, low.at[0:h], self.first, 1)
            self.landed(1, high)
            self.send(3, high.at[h : 2 * h], self.first, -1)
            self.across(1)
            self.across(2)

        def turn(self):
            h = self.half
            far = self.x.at[self.s, self.at(3)]
            self.landed(2, far.at[0:h])
            self.landed(3, far.at[h : 2 * h])
            self.across(3)

        def relay(self, k):
            h, fk = self.half, self.at(k)
            low, high = self.x.at[shifted(self.s, -1), fk], self.x.at[shifted(self.s, 1), fk]
            self.landed(4 + 2 * k, low)
            self.send(12 + 2 * k, low.at[0:h], self.second, 1)
            self.landed(5 + 2 * k, high)
            self.send(13 + 2 * k, high.at[h : 2 * h], self.second, -1)

        def complete(self):
            h, far = self.half, shifted(self.s, 2)
            for k in (0, 1, 2, 3):
                place = self.x.at[far, self.at(k)]
                self.landed(12 + 2 * k, place.at[0:h])
                self.landed(13 + 2 * k, place.at[h : 2 * h])

    axes = [("x", "y"), ("x", "y"), ("y", "x"), ("y", "x")]
    gathers = [Gather(u, axes[u]) for u in range(UNITS)]
    reductions = [
        Reduction(
            axes[u], p_all.at[u], half_s.at[u], full_s.at[u], sums.at[u], half_f.at[u], full_f.at[u],
            r_send.at[u], r_recv.at[u],
        )
        for u in range(UNITS)
    ]

    def mlp(u):
        gathers[u].complete()
        flat = x_all[u].reshape(peers * rows, width)
        gate = contract_last(flat, wg[...])
        upward = contract_last(flat, wu[...])
        hidden = (gate / (1.0 + jnp.exp(-gate)) * upward).astype(BF16)
        step = min(512, width)
        for n in range(0, width, step):
            part = jnp.dot(hidden, wd[:, n : n + step], preferred_element_type=F32)
            p_all[u, :, :, :, n : n + step] = part.astype(BF16).reshape(RING, RING, rows, step)

    def giving_back(o):
        to = lax.rem(me + o, count)
        return remote(back_send.at[o], back.at[me], b_send.at[o], b_recv.at[me], (to, tp))

    def give_back(u):
        total = reductions[u].finish().astype(BF16)
        for j in range(per):
            o = u * per + j
            if o:
                back_send[o] = total[2 * j : 2 * j + 2, :]
            else:
                back[me] = total[0:2, :]
        for j in range(per):
            o = u * per + j
            if o:
                giving_back(o).start()

    early, late = (0, 3), (1, 2)
    for u in early:
        gathers[u].begin()
    for u in early:
        gathers[u].along()
    for u in early:
        gathers[u].relay(0)
    for u in early:
        gathers[u].turn()
    for k in (1, 2):
        for u in early:
            gathers[u].relay(k)
    for u in late:
        gathers[u].begin()
    for u in early:
        gathers[u].relay(3)
    for u in late:
        gathers[u].along()
    for u in late:
        gathers[u].relay(0)
    for copy in weight_copies:
        copy.wait()
    mlp(0)
    reductions[0].begin()
    for u in late:
        gathers[u].turn()
    mlp(3)
    reductions[3].begin()
    for k in (1, 2, 3):
        for u in late:
            gathers[u].relay(k)
    for k in (3, 1, 2, 0):
        for u in early:
            reductions[u].relay(k)
    mlp(1)
    reductions[1].begin()
    for u in early:
        reductions[u].turn()
    mlp(2)
    reductions[2].begin()
    for u in early:
        reductions[u].cross()
    for k in (3, 1, 2, 0):
        for u in late:
            reductions[u].relay(k)
    for u in early:
        give_back(u)
    for u in late:
        reductions[u].turn()
    for u in late:
        reductions[u].cross()
    for u in late:
        give_back(u)

    def came_back(step, carry):
        sender = lax.rem(me + step, count)
        remote(back.at[sender], back.at[sender], b_send.at[step], b_recv.at[sender], (me, tp)).wait_recv()
        return carry

    lax.fori_loop(1, count, came_back, 0)
    table = jnp.concatenate([back[expert] for expert in range(count)], axis=0)
    mixture = route_weight[0] * jnp.dot(picks[0], table, preferred_element_type=F32)
    mixture = mixture + route_weight[1] * jnp.dot(picks[1], table, preferred_element_type=F32)
    out_ref[...] = hid[...] + mixture

    def sent(step, carry):
        dispatch(step).wait_send()
        giving_back(step).wait_send()
        return carry

    lax.fori_loop(1, count, sent, 0)

    def columns_sent(step, carry):
        columns_to(step).wait_send()
        return carry

    lax.fori_loop(1, peers, columns_sent, 0)
    for copy in halo + started:
        copy.wait_send()


def local(
    queries, keys, values, sink_logit, out_weight, residual, norm_gain, routes, route_weights,
    gate_weight, up_weight, down_weight,
):
    count = lax.axis_size("sp")
    tokens, width = residual.shape
    length, kv = keys.shape
    inner = gate_weight.shape[2]
    heads = queries.shape[1]
    rows = 2 * count // UNITS
    half = rows // 2
    vmem = pl.BlockSpec(memory_space=pltpu.VMEM)
    smem = pl.BlockSpec(memory_space=pltpu.SMEM)
    hbm = pl.BlockSpec(memory_space=pl.ANY)
    dma = pltpu.SemaphoreType.DMA

    def reduction_buffers(units, tall, wide):
        return [
            pltpu.VMEM((units, RING, RING, tall, wide), BF16),
            pltpu.VMEM((units, 2, RING, tall // 2, wide), BF16),
            pltpu.VMEM((units, 2, RING, tall, wide), BF16),
            pltpu.VMEM((units, RING, tall, wide), BF16),
            pltpu.VMEM((units, 2, tall // 2, wide), BF16),
            pltpu.VMEM((units, 2, tall, wide), BF16),
        ]

    out = pl.pallas_call(
        functools.partial(kernel, count),
        out_shape=jax.ShapeDtypeStruct((tokens, width), F32),
        in_specs=[vmem, vmem, vmem, smem, vmem, vmem, vmem, vmem, vmem, hbm, hbm, hbm],
        out_specs=vmem,
        scratch_shapes=[
            pltpu.VMEM((inner, width), BF16),
            pltpu.VMEM((inner, width), BF16),
            pltpu.VMEM((inner, width), BF16),
            pltpu.VMEM((kv, length + 2 * WINDOW), BF16),
            pltpu.VMEM((kv, length + 2 * WINDOW), BF16),
            pltpu.VMEM((heads, width), BF16),
            pltpu.VMEM((length, heads), BF16),
            pltpu.VMEM((tokens, width), F32),
            pltpu.VMEM((count, 2, width), BF16),
            pltpu.VMEM((count, 2, width), BF16),
            pltpu.VMEM((UNITS, RING, RING, rows, width), BF16),
            *reduction_buffers(UNITS, rows, width),
            *reduction_buffers(2, tokens, width // 2),
            pltpu.VMEM((count, 2, width), BF16),
            pltpu.VMEM((count, 2, width), BF16),
            dma((3,)),
            dma((4,)),
            dma((4,)),
            dma((RING * RING,)),
            dma((RING * RING,)),
            dma((count,)),
            dma((count,)),
            dma((count,)),
            dma((count,)),
            dma((UNITS, 20)),
            dma((UNITS, 20)),
            dma((UNITS, 20)),
            dma((UNITS, 20)),
            dma((2, 20)),
            dma((2, 20)),
        ],
        compiler_params=pltpu.CompilerParams(
            collective_id=0, has_side_effects=True, vmem_limit_bytes=60 * 1024 * 1024
        ),
        name="layer",
    )(
        queries, keys.T, values.T, sink_logit, out_weight, residual, norm_gain.reshape(1, width), routes.T,
        route_weights.T, jnp.swapaxes(gate_weight, 1, 2), jnp.swapaxes(up_weight, 1, 2), down_weight,
    )
    return out.astype(BF16)


def solution(mesh):
    in_specs = (
        P("sp", "tp"),
        P("sp", "tp"),
        P("sp", "tp"),
        P("tp"),
        P(None, "tp"),
        P(("sp", "tp"), None),
        P(),
        P(("sp", "tp"), None),
        P(("sp", "tp"), None),
        P("sp", None, "tp"),
        P("sp", None, "tp"),
        P("sp", "tp", None),
    )
    out_specs = P(("sp", "tp"), None)
    return jax.shard_map(local, mesh=mesh, in_specs=in_specs, out_specs=out_specs, check_vma=False)
```

time: 273 us -> 118 us (0.43)
  Pallas kernels: 0 us -> 116 us
  waiting for transfers between devices: 99.2 us -> 0 us
  blocking collectives: 95.6 us -> 0 us
  starting transfers between devices: 33.5 us -> 0 us
  local copies, waits for them, and re-layouts: 14.5 us -> 0 us
  between operations: 13.8 us -> 0.01 us
  matrix products: 10.9 us -> 0 us
  other arithmetic: 4.35 us -> 1.54 us
    pallas_call x0 -> x1, Pallas kernels: none -> 116 us  [local(): pl.pallas_call(functools.partial(kernel, count), out_shape=jax.ShapeDtype...]
    all_to_all x2 -> x0, blocking collectives: 95.6 us -> none  [the longest x1 54.8 us: summed_on_arrival(): lax.all_to_all(tiles, axis, split_axis=0, concat_axis=0, tiled=True)]
    all_gather x1 -> x0, waiting for transfers between devices: 54.4 us -> none  [local(): lax.all_gather(lax.all_to_all(sending, 'sp', split_axis=0, concat_axis=0,...]
    all_to_all x3 -> x0, waiting for transfers between devices: 44.8 us -> none  [the longest x1 22.2 us: local(): lax.all_to_all(summed_on_arrival(partial_value.astype(jnp.bfloat16), 'tp'...]
    all_to_all x3 -> x0, starting transfers between devices: 23.4 us -> none  [the longest x1 14.3 us: local(): lax.all_to_all(summed_on_arrival(partial_value.astype(jnp.bfloat16), 'tp'...]
    dot_general x9 -> x0, matrix products: 10.9 us -> none  [the longest x1 4 us: local(): gate = jnp.dot(flat, gate_weight[0], preferred_element_type=jnp.float32)]
    ppermute x2 -> x0, starting transfers between devices: 10 us -> none  [the longest x1 5.11 us: with_halo(): lax.ppermute(lax.slice_in_dim(block, 0, width, axis=dim), axis, backward)]
    reshape x7 -> x0, local copies, waits for them, and re-layouts: 8.49 us -> none  [the longest x1 7.26 us: local(): flat = piece.reshape(-1, piece.shape[-1])]
  transfers between devices with their start and end apart: 6 -> 0, of which waited for: 4 -> 0; matrix products, arithmetic and copies ran while one was open for 1% -> 0% of each run, Pallas kernels for 0% -> 0%
where the time goes in v2:
time: 118 us
  Pallas kernels  116 us (98%)
  other arithmetic  1.54 us (1%)
    pallas_call x1, Pallas kernels, local(): pl.pallas_call(functools.partial(kernel, count), out_shape=jax.ShapeDtype...  116 us

profile of v2, /device:TPU:1, one launch (start us, length us, event | category | flops | bytes accessed | tf_op | source)
XLA Modules:
  0.0 118.0 jit_solution(56795720503264443)
XLA Ops:
  0.0 116.4 %layer.1 = f32[16,2048]{1,0:T(8,128)} custom-call(bf16[256,128]{1,0:T(8,128)(2,1)} %q_ref.1, bf16[64,256]{1,0:T(8,128)(2,1)} %bitcast.9, bf16[64,256]{1,0:T(8,128)(2,1)} %bitcast.10, f32[2]{0:T(128)} %sink_ref.1, bf16[2048,128]{1,0:T(8,128)(2,1)} %w_ref.1, bf16[16,2048]{1,0:T(8,128)(2,1)} %res_ref.1, f32[1,2048]{1,0:T(1,128)} %bitcast.11, s32[2,16]{1,0:T(2,128)} %bitcast.12, ...), custom_call_target="tpu_custom_call" | custom-call | tf_op jit(solution)/shard_map/layer/pallas_call | solution.py:518
  116.4 1.5 %convert_element_type.3 = bf16[16,2048]{1,0:T(8,128)(2,1)} convert(f32[16,2048]{1,0:T(8,128)} %layer.1) | non-fusion elementwise | flops 32768 | bytes 196608 | tf_op jit(solution)/shard_map/convert_element_type | solution.py:563

commit v3 on v0

v3 whole, which is shorter than its diff:
```python
import functools

import jax
import jax.numpy as jnp
from jax import lax
from jax.experimental import pallas as pl
from jax.experimental.pallas import tpu as pltpu
from jax.sharding import PartitionSpec as P

HEADS = 32
KV_HEADS = 16
HEAD = 64
WINDOW = 128
EPS = 1e-06
NEGATIVE = -1e30

UNITS = 4
RING = 4
MESH = pl.DeviceIdType.MESH
BF16 = jnp.bfloat16
F32 = jnp.float32


def remote(src, dst, send_sem, recv_sem, device):
    return pltpu.make_async_remote_copy(
        src_ref=src, dst_ref=dst, send_sem=send_sem, recv_sem=recv_sem, device_id=device, device_id_type=MESH
    )


def contract_last(a, b):
    return lax.dot_general(a, b, (((1,), (1,)), ((), ())), preferred_element_type=F32)


def kernel(
    count,
    q_in, kt_in, vt_in, sink_in, w_in, res_in, gain_in, routes_in, rw_in, wg_in, wu_in, wd_in,
    out_ref,
    q_ref, kt_ref, vt_ref, sink_ref, w_ref, res_ref, gain_ref, routes_ref, rw_ref, wg, wu, wd,
    k_ext, v_ext, attn_all, cols, proj,
    sending, arrived, x_all, p_all, half_s, full_s, sums, half_f, full_f, back_send, back,
    in_sem, h_send, h_recv, a_send, a_recv, o_send, o_recv, d_send, d_recv, b_send, b_recv, g_send, g_recv, r_send, r_recv,
):
    me = lax.axis_index("sp")
    tp = lax.axis_index("tp")
    peers = RING * RING
    ty, tx = tp // RING, lax.rem(tp, RING)
    spot = {"x": tx, "y": ty}
    rows = 2 * count // UNITS
    per = count // UNITS
    tokens, width = proj.shape
    length = q_ref.shape[0]
    groups = length // WINDOW

    def shifted(pos, delta):
        return lax.rem(pos + (delta + RING), RING)

    def near(axis, delta):
        if axis == "x":
            return (me, ty * RING + shifted(tx, delta))
        return (me, shifted(ty, delta) * RING + tx)

    barrier = pltpu.get_barrier_semaphore()

    def greet_sp(step, carry):
        pl.semaphore_signal(barrier, inc=1, device_id=(lax.rem(me + step, count), tp), device_id_type=MESH)
        return carry

    def greet_tp(step, carry):
        pl.semaphore_signal(barrier, inc=1, device_id=(me, lax.rem(tp + step, peers)), device_id_type=MESH)
        return carry

    lax.fori_loop(1, count, greet_sp, 0)
    lax.fori_loop(1, peers, greet_tp, 0)

    pairs = [
        (kt_in, kt_ref), (vt_in, vt_ref), (q_in, q_ref), (sink_in, sink_ref), (routes_in, routes_ref), (rw_in, rw_ref),
        (w_in, w_ref), (res_in, res_ref), (gain_in, gain_ref), (wg_in.at[0], wg), (wu_in.at[0], wu), (wd_in.at[0], wd),
    ]
    loads = [pltpu.make_async_copy(src, dst, in_sem.at[i]) for i, (src, dst) in enumerate(pairs)]
    for copy in loads:
        copy.start()
    for copy in loads[:4]:
        copy.wait()
    k_ext[:, WINDOW : WINDOW + length] = kt_ref[...]
    v_ext[:, WINDOW : WINDOW + length] = vt_ref[...]
    pl.semaphore_wait(barrier, count - 1 + peers - 1)

    right, left = lax.rem(me + 1, count), lax.rem(me + count - 1, count)
    for own, ext in ((kt_ref, k_ext), (vt_ref, v_ext)):
        remote(
            own.at[:, length - WINDOW : length], ext.at[:, 0:WINDOW], h_send.at[0], h_recv.at[0], (right, tp)
        ).start()
        remote(
            own.at[:, 0:WINDOW], ext.at[:, WINDOW + length : 2 * WINDOW + length], h_send.at[0], h_recv.at[0], (left, tp)
        ).start()
    halo = remote(k_ext, k_ext, h_send.at[0], h_recv.at[0], (me, tp))
    halo.wait_recv()

    class Gather:
        def __init__(self, blocks, base, axes, send_sem, recv_sem):
            self.blocks, self.base = blocks, base
            self.first, self.second = axes
            self.f, self.s = spot[self.first], spot[self.second]
            self.half = blocks.shape[1] // 2
            self.send_sem, self.recv_sem = send_sem, recv_sem

        def place(self, s, k):
            return self.base + s * RING + shifted(self.f, (0, -1, 1, 2)[k])

        def block(self, s, k):
            return self.blocks.at[self.place(s, k)]

        def send(self, number, ref, axis, delta):
            remote(ref, ref, self.send_sem, self.recv_sem.at[number], near(axis, delta)).start()

        def landed(self, number, ref):
            remote(ref, ref, self.send_sem, self.recv_sem.at[number], near("x", 1)).wait_recv()

        def begin(self):
            own = self.block(self.s, 0)
            self.send(0, own, self.first, 1)
            self.send(1, own, self.first, -1)

        def across(self, k):
            own = self.block(self.s, k)
            self.send(3 + k, own, self.second, 1)
            self.send(3 + k, own, self.second, -1)

        def along(self):
            h = self.half
            low, high = self.block(self.s, 1), self.block(self.s, 2)
            self.landed(0, low)
            self.send(2, low.at[0:h], self.first, 1)
            self.landed(1, high)
            self.send(2, high.at[h : 2 * h], self.first, -1)

        def turn(self):
            self.landed(2, self.block(self.s, 3))
            self.across(3)

        def relay(self, k):
            h = self.half
            low, high = self.block(shifted(self.s, -1), k), self.block(shifted(self.s, 1), k)
            self.landed(3 + k, self.blocks.at[0:2])
            self.send(7, low.at[0:h], self.second, 1)
            self.send(7, high.at[h : 2 * h], self.second, -1)

        def complete(self):
            self.landed(7, self.blocks.at[0:RING])

    orders = [("x", "y"), ("y", "x")]
    attended = [Gather(attn_all, n * peers, orders[n], a_send.at[0], a_recv.at[n]) for n in range(groups)]

    row_i = lax.broadcasted_iota(jnp.int32, (WINDOW, 3 * WINDOW), 0)
    col_j = lax.broadcasted_iota(jnp.int32, (WINDOW, 3 * WINDOW), 1)
    close = (col_j >= row_i) & (col_j <= row_i + 2 * WINDOW)
    for n in range(groups):
        position = me * length + (n - 1) * WINDOW + col_j
        valid = close & (position >= 0) & (position < length * count)
        band = slice(n * WINDOW, (n + 3) * WINDOW)
        for r in range(HEADS // KV_HEADS):
            query = q_ref[n * WINDOW : (n + 1) * WINDOW, r * HEAD : (r + 1) * HEAD]
            scores = jnp.dot(query, k_ext[:, band], preferred_element_type=F32) * HEAD ** (-0.5)
            sink = jnp.full((WINDOW, 1), sink_ref[r], F32)
            masked = jnp.where(valid, scores, NEGATIVE)
            top = jnp.maximum(jnp.max(masked, axis=-1, keepdims=True), sink)
            probs = jnp.exp(masked - top)
            denom = jnp.sum(probs, axis=-1, keepdims=True) + jnp.exp(sink - top)
            weights = (probs / denom).astype(BF16)
            attn_all[attended[n].place(attended[n].s, 0), :, r * HEAD : (r + 1) * HEAD] = contract_last(
                weights, v_ext[:, band]
            ).astype(BF16)
        attended[n].begin()
    for part in attended:
        part.across(0)

    for copy in loads[4:9]:
        copy.wait()
    t_row = lax.broadcasted_iota(jnp.int32, (tokens, tokens), 0)
    t_col = lax.broadcasted_iota(jnp.int32, (tokens, tokens), 1)

    def as_column(row):
        spread = jnp.where(t_row == t_col, jnp.broadcast_to(row, (tokens, tokens)), 0.0)
        return jnp.sum(spread, axis=1, keepdims=True)

    named = [routes_ref[a : a + 1, :].astype(F32) for a in range(2)]
    named_column = [as_column(row) for row in named]
    slot = []
    for row in named:
        rank = jnp.zeros((1, tokens), F32)
        for column in named_column:
            same = (column == row) & (t_row < t_col)
            rank = rank + jnp.sum(jnp.where(same, 1.0, 0.0), axis=0, keepdims=True)
        slot.append(2.0 * row + rank)
    slot_down = lax.broadcasted_iota(jnp.int32, (2 * count, tokens), 0).astype(F32)
    slot_across = lax.broadcasted_iota(jnp.int32, (tokens, 2 * count), 1).astype(F32)
    placed = jnp.where((slot_down == slot[0]) | (slot_down == slot[1]), 1.0, 0.0).astype(BF16)
    picks = [jnp.where(slot_across == as_column(row), 1.0, 0.0).astype(BF16) for row in slot]
    route_weight = [as_column(rw_ref[a : a + 1, :]) for a in range(2)]

    def both(items, *stages):
        for name, *given in stages:
            for item in items:
                getattr(item, name)(*given)

    both(
        attended, ("along",), ("across", 1), ("across", 2), ("relay", 0), ("turn",), ("relay", 1), ("relay", 2),
        ("relay", 3), ("complete",),
    )

    for n in range(groups):
        ys = [(t // RING, t % RING) if n == 0 else (t % RING, t // RING) for t in range(peers)]
        joined = jnp.concatenate([attn_all[n * peers + i * RING + j] for i, j in ys], axis=1)
        cols[n * WINDOW : (n + 1) * WINDOW, :] = jnp.dot(
            joined, w_ref[...], preferred_element_type=F32
        ).astype(BF16)
    own_columns = pl.ds(pl.multiple_of(tp * WINDOW, WINDOW), WINDOW)

    def rows_to(step, carry):
        to = lax.rem(tp + step, peers)
        remote(
            cols.at[pl.ds(pl.multiple_of(to * tokens, tokens), tokens), :], proj.at[:, own_columns],
            o_send.at[0], o_recv.at[0], (me, to),
        ).start()
        return carry

    lax.fori_loop(1, peers, rows_to, 0)
    proj[:, own_columns] = cols[pl.ds(pl.multiple_of(tp * tokens, tokens), tokens), :]
    others = proj.at[:, 0 : (peers - 1) * WINDOW]
    exchanged = remote(others, others, o_send.at[0], o_recv.at[0], (me, tp))
    exchanged.wait_recv()

    hidden_state = res_ref[...].astype(F32) + proj[...].astype(F32)
    inverse = lax.rsqrt(jnp.mean(hidden_state * hidden_state, axis=-1, keepdims=True) + EPS)
    normed = (hidden_state * inverse * gain_ref[...]).astype(BF16)
    slots = jnp.dot(placed, normed, preferred_element_type=F32).astype(BF16)
    for expert in range(count):
        sending[expert] = slots[2 * expert : 2 * expert + 2, :]

    def dispatch(step):
        to = lax.rem(me + step, count)
        remote(
            sending.at[to], arrived.at[count - step], d_send.at[0], d_recv.at[(count - step) // per], (to, tp)
        ).start()

    def dispatch_pair(step, carry):
        dispatch(step)
        dispatch(count - step)
        return carry

    lax.fori_loop(1, count // 2, dispatch_pair, 0)
    dispatch(count // 2)
    arrived[0] = sending[me]

    class Reduction:
        def __init__(self, unit, axes):
            self.first, self.second = axes
            self.f, self.s = spot[self.first], spot[self.second]
            self.parts, self.hs, self.fs = p_all.at[unit], half_s.at[unit], full_s.at[unit]
            self.total, self.hf, self.ff = sums.at[unit], half_f.at[unit], full_f.at[unit]
            self.recv_sem = r_recv.at[unit]

        def send(self, number, src, dst, axis, delta):
            remote(src, dst, r_send.at[0], self.recv_sem.at[number], near(axis, delta)).start()

        def landed(self, number, ref):
            remote(ref, ref, r_send.at[0], self.recv_sem.at[number], near("x", 1)).wait_recv()

        def at(self, k):
            return shifted(self.f, (0, -1, 1, 2)[k])

        def begin(self):
            h, far = rows // 2, shifted(self.s, 2)
            for k in (3, 1, 2, 0):
                src = self.parts.at[far, self.at(k)]
                self.send(k, src.at[0:h], self.hs.at[k, 0], self.second, 1)
                self.send(k, src.at[h:rows], self.hs.at[k, 1], self.second, -1)

        def relay(self, k):
            h, fk = rows // 2, self.at(k)
            up, down = shifted(self.s, 1), shifted(self.s, -1)
            self.landed(k, self.hs.at[k])
            self.parts[up, fk, 0:h] = (self.parts[up, fk, 0:h].astype(F32) + self.hs[k, 0].astype(F32)).astype(BF16)
            self.send(4 + k, self.parts.at[up, fk], self.fs.at[k, 0], self.second, 1)
            self.parts[down, fk, h:rows] = (
                self.parts[down, fk, h:rows].astype(F32) + self.hs[k, 1].astype(F32)
            ).astype(BF16)
            self.send(4 + k, self.parts.at[down, fk], self.fs.at[k, 1], self.second, -1)

        def summed(self, k):
            self.landed(4 + k, self.fs.at[k])
            return self.parts[self.s, self.at(k)].astype(F32) + self.fs[k, 0].astype(F32) + self.fs[k, 1].astype(F32)

        def turn(self):
            h = rows // 2
            self.total[3] = self.summed(3).astype(BF16)
            self.send(8, self.total.at[3, 0:h], self.hf.at[0], self.first, 1)
            self.send(9, self.total.at[3, h:rows], self.hf.at[1], self.first, -1)

        def cross(self):
            h = rows // 2
            high = self.summed(2)
            self.landed(8, self.hf.at[0])
            self.total[2, 0:h] = (high[0:h] + self.hf[0].astype(F32)).astype(BF16)
            self.total[2, h:rows] = high[h:].astype(BF16)
            self.send(10, self.total.at[2], self.ff.at[0], self.first, 1)
            low = self.summed(1)
            self.landed(9, self.hf.at[1])
            self.total[1, 0:h] = low[0:h].astype(BF16)
            self.total[1, h:rows] = (low[h:] + self.hf[1].astype(F32)).astype(BF16)
            self.send(10, self.total.at[1], self.ff.at[1], self.first, -1)

        def finish(self):
            own = self.summed(0)
            self.landed(10, self.ff)
            return own + self.ff[0].astype(F32) + self.ff[1].astype(F32)

    axes = [orders[0], orders[0], orders[1], orders[1]]
    gathers = [Gather(x_all, u * peers, axes[u], g_send.at[0], g_recv.at[u]) for u in range(UNITS)]
    reductions = [Reduction(u, axes[u]) for u in range(UNITS)]

    def rows_here(u):
        first = 1 if u == 0 else 0
        region = arrived.at[u * per + first : (u + 1) * per]
        remote(region, region, d_send.at[0], d_recv.at[u], (me, tp)).wait_recv()
        place = gathers[u].place(gathers[u].s, 0)
        for j in range(per):
            x_all[place, 2 * j : 2 * j + 2, :] = arrived[u * per + j]

    held = {}

    def mlp_up(u):
        gathers[u].complete()
        flat = x_all[u * peers : (u + 1) * peers].reshape(peers * rows, width)
        gate = contract_last(flat, wg[...])
        upward = contract_last(flat, wu[...])
        held[u] = (gate / (1.0 + jnp.exp(-gate)) * upward).astype(BF16)

    def mlp_down(u):
        step = min(512, width)
        for n in range(0, width, step):
            part = jnp.dot(held[u], wd[:, n : n + step], preferred_element_type=F32)
            p_all[u, :, :, :, n : n + step] = part.astype(BF16).reshape(RING, RING, rows, step)

    def give_back(u):
        total = reductions[u].finish().astype(BF16)
        for j in range(per):
            o = u * per + j
            if o:
                back_send[o] = total[2 * j : 2 * j + 2, :]
            else:
                back[me] = total[0:2, :]
        for j in range(per):
            o = u * per + j
            if o:
                remote(
                    back_send.at[o], back.at[me], b_send.at[0], b_recv.at[0], (lax.rem(me + o, count), tp)
                ).start()

    early = [gathers[0], gathers[3]]
    late = [gathers[1], gathers[2]]
    for u in (0, 3):
        rows_here(u)
        gathers[u].begin()
    both(early, ("across", 0), ("along",), ("across", 1), ("across", 2), ("relay", 0), ("turn",), ("relay", 1), ("relay", 2))
    for u in (1, 2):
        rows_here(u)
        gathers[u].begin()
    both(late, ("across", 0))
    both(early, ("relay", 3))
    both(late, ("along",), ("across", 1), ("across", 2))
    for copy in loads[9:]:
        copy.wait()
    mlp_up(0)
    both(late, ("relay", 0))
    mlp_down(0)
    reductions[0].begin()
    both(late, ("turn",))
    mlp_up(3)
    both(late, ("relay", 1))
    mlp_down(3)
    reductions[3].begin()
    both(late, ("relay", 2), ("relay", 3))
    for k in (3, 1, 2, 0):
        reductions[0].relay(k)
    mlp_up(1)
    mlp_down(1)
    reductions[1].begin()
    for k in (3, 1, 2, 0):
        reductions[3].relay(k)
    reductions[0].turn()
    mlp_up(2)
    mlp_down(2)
    reductions[2].begin()
    reductions[3].turn()
    for k in (3, 1, 2, 0):
        reductions[1].relay(k)
    reductions[0].cross()
    reductions[3].cross()
    for k in (3, 1, 2, 0):
        reductions[2].relay(k)
    give_back(0)
    give_back(3)
    reductions[1].turn()
    reductions[2].turn()
    reductions[1].cross()
    reductions[2].cross()
    give_back(1)
    give_back(2)

    from_others = back.at[0 : count - 1]
    returned = remote(from_others, from_others, b_send.at[0], b_recv.at[0], (me, tp))
    returned.wait_recv()
    table = jnp.concatenate([back[expert] for expert in range(count)], axis=0)
    mixture = route_weight[0] * jnp.dot(picks[0], table, preferred_element_type=F32)
    mixture = mixture + route_weight[1] * jnp.dot(picks[1], table, preferred_element_type=F32)
    out_ref[...] = hidden_state + mixture

    returned.wait_send()
    dispatched = sending.at[0 : count - 1]
    remote(dispatched, dispatched, d_send.at[0], b_recv.at[0], (me, tp)).wait_send()
    exchanged.wait_send()
    halo.wait_send()
    sent = attn_all.at[0 : groups * (peers - 1)]
    remote(sent, sent, a_send.at[0], b_recv.at[0], (me, tp)).wait_send()
    sent = x_all.at[0 : UNITS * (peers - 1)]
    remote(sent, sent, g_send.at[0], b_recv.at[0], (me, tp)).wait_send()
    remote(sent, sent, r_send.at[0], b_recv.at[0], (me, tp)).wait_send()


def local(
    queries, keys, values, sink_logit, out_weight, residual, norm_gain, routes, route_weights,
    gate_weight, up_weight, down_weight,
):
    count = lax.axis_size("sp")
    tokens, width = residual.shape
    length, kv = keys.shape
    inner = gate_weight.shape[2]
    heads = queries.shape[1]
    rows = 2 * count // UNITS
    half = rows // 2
    groups = length // WINDOW
    peers = RING * RING
    dma = pltpu.SemaphoreType.DMA
    given = (
        queries, keys.T, values.T, sink_logit, out_weight, residual, norm_gain.reshape(1, width), routes.T,
        route_weights.T, jnp.swapaxes(gate_weight, 1, 2), jnp.swapaxes(up_weight, 1, 2), down_weight,
    )
    held = [pltpu.VMEM(a.shape, a.dtype) for a in given[:9]] + [pltpu.VMEM((inner, width), BF16)] * 3
    held[3] = pltpu.SMEM(sink_logit.shape, F32)
    out = pl.pallas_call(
        functools.partial(kernel, count),
        out_shape=jax.ShapeDtypeStruct((tokens, width), F32),
        in_specs=[pl.BlockSpec(memory_space=pl.ANY)] * len(given),
        out_specs=pl.BlockSpec(memory_space=pltpu.VMEM),
        scratch_shapes=[
            *held,
            pltpu.VMEM((kv, length + 2 * WINDOW), BF16),
            pltpu.VMEM((kv, length + 2 * WINDOW), BF16),
            pltpu.VMEM((groups * peers, WINDOW, heads), BF16),
            pltpu.VMEM((length, heads), BF16),
            pltpu.VMEM((tokens, width), BF16),
            pltpu.VMEM((count, 2, width), BF16),
            pltpu.VMEM((count, 2, width), BF16),
            pltpu.VMEM((UNITS * peers, rows, width), BF16),
            pltpu.VMEM((UNITS, RING, RING, rows, width), BF16),
            pltpu.VMEM((UNITS, RING, 2, half, width), BF16),
            pltpu.VMEM((UNITS, RING, 2, rows, width), BF16),
            pltpu.VMEM((UNITS, RING, rows, width), BF16),
            pltpu.VMEM((UNITS, 2, half, width), BF16),
            pltpu.VMEM((UNITS, 2, rows, width), BF16),
            pltpu.VMEM((count, 2, width), BF16),
            pltpu.VMEM((count, 2, width), BF16),
            dma((len(given),)),
            dma((1,)),
            dma((1,)),
            dma((1,)),
            dma((groups, 8)),
            dma((1,)),
            dma((1,)),
            dma((1,)),
            dma((UNITS,)),
            dma((1,)),
            dma((1,)),
            dma((1,)),
            dma((UNITS, 8)),
            dma((1,)),
            dma((UNITS, 11)),
        ],
        compiler_params=pltpu.CompilerParams(
            collective_id=0, has_side_effects=True, vmem_limit_bytes=60 * 1024 * 1024
        ),
        name="layer",
    )(*given)
    return out.astype(BF16)


def solution(mesh):
    in_specs = (
        P("sp", "tp"),
        P("sp", "tp"),
        P("sp", "tp"),
        P("tp"),
        P(None, "tp"),
        P(("sp", "tp"), None),
        P(),
        P(("sp", "tp"), None),
        P(("sp", "tp"), None),
        P("sp", None, "tp"),
        P("sp", None, "tp"),
        P("sp", "tp", None),
    )
    out_specs = P(("sp", "tp"), None)
    return jax.shard_map(local, mesh=mesh, in_specs=in_specs, out_specs=out_specs, check_vma=False)
```

time: 273 us -> 114 us (0.42)
  Pallas kernels: 0 us -> 112 us
  waiting for transfers between devices: 99.2 us -> 0 us
  blocking collectives: 95.6 us -> 0 us
  starting transfers between devices: 33.5 us -> 0 us
  local copies, waits for them, and re-layouts: 14.5 us -> 0 us
  between operations: 13.8 us -> 0.01 us
  matrix products: 10.9 us -> 0 us
  other arithmetic: 4.35 us -> 1.54 us
    pallas_call x0 -> x1, Pallas kernels: none -> 112 us  [local(): pl.pallas_call(functools.partial(kernel, count), out_shape=jax.ShapeDtype...]
    all_to_all x2 -> x0, blocking collectives: 95.6 us -> none  [the longest x1 54.8 us: summed_on_arrival(): lax.all_to_all(tiles, axis, split_axis=0, concat_axis=0, tiled=True)]
    all_gather x1 -> x0, waiting for transfers between devices: 54.4 us -> none  [local(): lax.all_gather(lax.all_to_all(sending, 'sp', split_axis=0, concat_axis=0,...]
    all_to_all x3 -> x0, waiting for transfers between devices: 44.8 us -> none  [the longest x1 22.2 us: local(): lax.all_to_all(summed_on_arrival(partial_value.astype(jnp.bfloat16), 'tp'...]
    all_to_all x3 -> x0, starting transfers between devices: 23.4 us -> none  [the longest x1 14.3 us: local(): lax.all_to_all(summed_on_arrival(partial_value.astype(jnp.bfloat16), 'tp'...]
    dot_general x9 -> x0, matrix products: 10.9 us -> none  [the longest x1 4 us: local(): gate = jnp.dot(flat, gate_weight[0], preferred_element_type=jnp.float32)]
    ppermute x2 -> x0, starting transfers between devices: 10 us -> none  [the longest x1 5.11 us: with_halo(): lax.ppermute(lax.slice_in_dim(block, 0, width, axis=dim), axis, backward)]
    reshape x7 -> x0, local copies, waits for them, and re-layouts: 8.49 us -> none  [the longest x1 7.26 us: local(): flat = piece.reshape(-1, piece.shape[-1])]
  transfers between devices with their start and end apart: 6 -> 0, of which waited for: 4 -> 0; matrix products, arithmetic and copies ran while one was open for 1% -> 0% of each run, Pallas kernels for 0% -> 0%
where the time goes in v3:
time: 114 us
  Pallas kernels  112 us (98%)
  other arithmetic  1.54 us (1%)
    pallas_call x1, Pallas kernels, local(): pl.pallas_call(functools.partial(kernel, count), out_shape=jax.ShapeDtype...  112 us

profile of v3, /device:TPU:1, one launch (start us, length us, event | category | flops | bytes accessed | tf_op | source)
XLA Modules:
  0.0 113.9 jit_solution(957415498337654299)
XLA Ops:
  0.0 112.3 %layer.1 = f32[16,2048]{1,0:T(8,128)} custom-call(bf16[256,128]{1,0:T(8,128)(2,1)} %q_in.1, bf16[64,256]{1,0:T(8,128)(2,1)} %bitcast.9, bf16[64,256]{1,0:T(8,128)(2,1)} %bitcast.10, f32[2]{0:T(128)} %sink_in.1, bf16[2048,128]{1,0:T(8,128)(2,1)} %w_in.1, bf16[16,2048]{1,0:T(8,128)(2,1)} %res_in.1, f32[1,2048]{1,0:T(1,128)} %bitcast.11, s32[2,16]{1,0:T(2,128)} %bitcast.12, ...), custom_call_target="tpu_custom_call" | custom-call | tf_op jit(solution)/shard_map/layer/pallas_call | solution.py:451
  112.3 1.5 %convert_element_type.3 = bf16[16,2048]{1,0:T(8,128)(2,1)} convert(f32[16,2048]{1,0:T(8,128)} %layer.1) | non-fusion elementwise | flops 32768 | bytes 196608 | tf_op jit(solution)/shard_map/convert_element_type | solution.py:495

commit v4 on v3

--- a/solution.py
+++ b/solution.py
@@ -14,8 +14,16 @@
 EPS = 1e-06
 NEGATIVE = -1e30
 
-UNITS = 4
+UNITS = 8
 RING = 4
+ORDER = (
+    (0, 0), (0, 1), (1, 0), (0, 2), (0, 3), (0, 4), (0, 5), (1, 1), (2, 0), (0, 6), (1, 2), (1, 3), (3, 0), (2, 1),
+    (1, 4), (0, 7), (1, 5), (1, 6), (2, 2), (0, 8), (2, 3), (3, 1), (2, 4), (2, 5), (3, 2), (1, 7), (2, 6), (3, 3),
+    (1, 8), (1, 9), (3, 4), (0, 9), (3, 5), (2, 7), (3, 6), (1, 10), (2, 8), (2, 9), (1, 11), (1, 12), (1, 13),
+    (2, 10), (1, 14), (2, 11), (2, 12), (3, 7), (2, 13), (3, 8), (2, 14), (1, 15), (3, 9), (0, 10), (2, 15), (1, 16),
+    (3, 10), (3, 11), (3, 12), (3, 13), (2, 16), (3, 14), (0, 11), (0, 12), (0, 13), (0, 14), (3, 15), (0, 15),
+    (3, 16), (0, 16),
+)
 MESH = pl.DeviceIdType.MESH
 BF16 = jnp.bfloat16
 F32 = jnp.float32
@@ -97,11 +105,10 @@
     halo.wait_recv()
 
     class Gather:
-        def __init__(self, blocks, base, axes, send_sem, recv_sem):
-            self.blocks, self.base = blocks, base
+        def __init__(self, blocks, base, axes, cut, send_sem, recv_sem):
+            self.blocks, self.base, self.cut = blocks, base, cut
             self.first, self.second = axes
             self.f, self.s = spot[self.first], spot[self.second]
-            self.half = blocks.shape[1] // 2
             self.send_sem, self.recv_sem = send_sem, recv_sem
 
         def place(self, s, k):
@@ -109,6 +116,13 @@
 
         def block(self, s, k):
             return self.blocks.at[self.place(s, k)]
+
+        def part(self, ref, which):
+            if self.cut == 0:
+                h = ref.shape[0] // 2
+                return ref.at[which * h : (which + 1) * h]
+            h = ref.shape[1] // 2
+            return ref.at[:, which * h : (which + 1) * h]
 
         def send(self, number, ref, axis, delta):
             remote(ref, ref, self.send_sem, self.recv_sem.at[number], near(axis, delta)).start()
@@ -127,29 +141,27 @@
             self.send(3 + k, own, self.second, -1)
 
         def along(self):
-            h = self.half
             low, high = self.block(self.s, 1), self.block(self.s, 2)
             self.landed(0, low)
-            self.send(2, low.at[0:h], self.first, 1)
+            self.send(2, self.part(low, 0), self.first, 1)
             self.landed(1, high)
-            self.send(2, high.at[h : 2 * h], self.first, -1)
+            self.send(2, self.part(high, 1), self.first, -1)
 
         def turn(self):
             self.landed(2, self.block(self.s, 3))
             self.across(3)
 
         def relay(self, k):
-            h = self.half
             low, high = self.block(shifted(self.s, -1), k), self.block(shifted(self.s, 1), k)
             self.landed(3 + k, self.blocks.at[0:2])
-            self.send(7, low.at[0:h], self.second, 1)
-            self.send(7, high.at[h : 2 * h], self.second, -1)
+            self.send(7, self.part(low, 0), self.second, 1)
+            self.send(7, self.part(high, 1), self.second, -1)
 
         def complete(self):
             self.landed(7, self.blocks.at[0:RING])
 
     orders = [("x", "y"), ("y", "x")]
-    attended = [Gather(attn_all, n * peers, orders[n], a_send.at[0], a_recv.at[n]) for n in range(groups)]
+    attended = [Gather(attn_all, n * peers, orders[n], 0, a_send.at[0], a_recv.at[n]) for n in range(groups)]
 
     row_i = lax.broadcasted_iota(jnp.int32, (WINDOW, 3 * WINDOW), 0)
     col_j = lax.broadcasted_iota(jnp.int32, (WINDOW, 3 * WINDOW), 1)
@@ -243,13 +255,18 @@
             sending.at[to], arrived.at[count - step], d_send.at[0], d_recv.at[(count - step) // per], (to, tp)
         ).start()
 
+    pairs = [(u, UNITS - 1 - u) for u in range(UNITS // 2)]
+    pairs = [pairs[0], *pairs[2:], pairs[1]]
+
     def dispatch_pair(step, carry):
-        dispatch(step)
+        dispatch(step + 1)
         dispatch(count - step)
         return carry
 
-    lax.fori_loop(1, count // 2, dispatch_pair, 0)
-    dispatch(count // 2)
+    for low, _ in pairs:
+        if low == 0:
+            dispatch(1)
+        lax.fori_loop(max(low * per, 1), (low + 1) * per, dispatch_pair, 0)
     arrived[0] = sending[me]
 
     class Reduction:
@@ -270,20 +287,22 @@
             return shifted(self.f, (0, -1, 1, 2)[k])
 
         def begin(self):
-            h, far = rows // 2, shifted(self.s, 2)
+            h, far = width // 2, shifted(self.s, 2)
             for k in (3, 1, 2, 0):
                 src = self.parts.at[far, self.at(k)]
-                self.send(k, src.at[0:h], self.hs.at[k, 0], self.second, 1)
-                self.send(k, src.at[h:rows], self.hs.at[k, 1], self.second, -1)
+                self.send(k, src.at[:, 0:h], self.hs.at[k, 0], self.second, 1)
+                self.send(k, src.at[:, h:width], self.hs.at[k, 1], self.second, -1)
 
         def relay(self, k):
-            h, fk = rows // 2, self.at(k)
+            h, fk = width // 2, self.at(k)
             up, down = shifted(self.s, 1), shifted(self.s, -1)
             self.landed(k, self.hs.at[k])
-            self.parts[up, fk, 0:h] = (self.parts[up, fk, 0:h].astype(F32) + self.hs[k, 0].astype(F32)).astype(BF16)
+            self.parts[up, fk, :, 0:h] = (
+                self.parts[up, fk, :, 0:h].astype(F32) + self.hs[k, 0].astype(F32)
+            ).astype(BF16)
             self.send(4 + k, self.parts.at[up, fk], self.fs.at[k, 0], self.second, 1)
-            self.parts[down, fk, h:rows] = (
-                self.parts[down, fk, h:rows].astype(F32) + self.hs[k, 1].astype(F32)
+            self.parts[down, fk, :, h:width] = (
+                self.parts[down, fk, :, h:width].astype(F32) + self.hs[k, 1].astype(F32)
             ).astype(BF16)
             self.send(4 + k, self.parts.at[down, fk], self.fs.at[k, 1], self.second, -1)
 
@@ -292,22 +311,22 @@
             return self.parts[self.s, self.at(k)].astype(F32) + self.fs[k, 0].astype(F32) + self.fs[k, 1].astype(F32)
 
         def turn(self):
-            h = rows // 2
+            h = width // 2
             self.total[3] = self.summed(3).astype(BF16)
-            self.send(8, self.total.at[3, 0:h], self.hf.at[0], self.first, 1)
-            self.send(9, self.total.at[3, h:rows], self.hf.at[1], self.first, -1)
+            self.send(8, self.total.at[3, :, 0:h], self.hf.at[0], self.first, 1)
+            self.send(9, self.total.at[3, :, h:width], self.hf.at[1], self.first, -1)
 
         def cross(self):
-            h = rows // 2
+            h = width // 2
             high = self.summed(2)
             self.landed(8, self.hf.at[0])
-            self.total[2, 0:h] = (high[0:h] + self.hf[0].astype(F32)).astype(BF16)
-            self.total[2, h:rows] = high[h:].astype(BF16)
+            self.total[2, :, 0:h] = (high[:, 0:h] + self.hf[0].astype(F32)).astype(BF16)
+            self.total[2, :, h:width] = high[:, h:].astype(BF16)
             self.send(10, self.total.at[2], self.ff.at[0], self.first, 1)
             low = self.summed(1)
             self.landed(9, self.hf.at[1])
-            self.total[1, 0:h] = low[0:h].astype(BF16)
-            self.total[1, h:rows] = (low[h:] + self.hf[1].astype(F32)).astype(BF16)
+            self.total[1, :, 0:h] = low[:, 0:h].astype(BF16)
+            self.total[1, :, h:width] = (low[:, h:] + self.hf[1].astype(F32)).astype(BF16)
             self.send(10, self.total.at[1], self.ff.at[1], self.first, -1)
 
         def finish(self):
@@ -315,8 +334,8 @@
             self.landed(10, self.ff)
             return own + self.ff[0].astype(F32) + self.ff[1].astype(F32)
 
-    axes = [orders[0], orders[0], orders[1], orders[1]]
-    gathers = [Gather(x_all, u * peers, axes[u], g_send.at[0], g_recv.at[u]) for u in range(UNITS)]
+    axes = [orders[2 * u // UNITS] for u in range(UNITS)]
+    gathers = [Gather(x_all, u * peers, axes[u], 1, g_send.at[0], g_recv.at[u]) for u in range(UNITS)]
     reductions = [Reduction(u, axes[u]) for u in range(UNITS)]
 
     def rows_here(u):
@@ -329,18 +348,23 @@
 
     held = {}
 
-    def mlp_up(u):
-        gathers[u].complete()
-        flat = x_all[u * peers : (u + 1) * peers].reshape(peers * rows, width)
+    def mlp_up(pair):
+        for u in pair:
+            gathers[u].complete()
+        flat = jnp.concatenate(
+            [x_all[u * peers : (u + 1) * peers].reshape(peers * rows, width) for u in pair], axis=0
+        )
         gate = contract_last(flat, wg[...])
         upward = contract_last(flat, wu[...])
-        held[u] = (gate / (1.0 + jnp.exp(-gate)) * upward).astype(BF16)
-
-    def mlp_down(u):
+        held[pair] = (gate / (1.0 + jnp.exp(-gate)) * upward).astype(BF16)
+
+    def mlp_down(pair):
         step = min(512, width)
         for n in range(0, width, step):
-            part = jnp.dot(held[u], wd[:, n : n + step], preferred_element_type=F32)
-            p_all[u, :, :, :, n : n + step] = part.astype(BF16).reshape(RING, RING, rows, step)
+            part = jnp.dot(held[pair], wd[:, n : n + step], preferred_element_type=F32)
+            for i, u in enumerate(pair):
+                block = part[i * peers * rows : (i + 1) * peers * rows].reshape(RING, RING, rows, step)
+                p_all[u, :, :, :, n : n + step] = block.astype(BF16)
 
     def give_back(u):
         total = reductions[u].finish().astype(BF16)
@@ -357,56 +381,36 @@
                     back_send.at[o], back.at[me], b_send.at[0], b_recv.at[0], (lax.rem(me + o, count), tp)
                 ).start()
 
-    early = [gathers[0], gathers[3]]
-    late = [gathers[1], gathers[2]]
-    for u in (0, 3):
-        rows_here(u)
-        gathers[u].begin()
-    both(early, ("across", 0), ("along",), ("across", 1), ("across", 2), ("relay", 0), ("turn",), ("relay", 1), ("relay", 2))
-    for u in (1, 2):
-        rows_here(u)
-        gathers[u].begin()
-    both(late, ("across", 0))
-    both(early, ("relay", 3))
-    both(late, ("along",), ("across", 1), ("across", 2))
     for copy in loads[9:]:
         copy.wait()
-    mlp_up(0)
-    both(late, ("relay", 0))
-    mlp_down(0)
-    reductions[0].begin()
-    both(late, ("turn",))
-    mlp_up(3)
-    both(late, ("relay", 1))
-    mlp_down(3)
-    reductions[3].begin()
-    both(late, ("relay", 2), ("relay", 3))
-    for k in (3, 1, 2, 0):
-        reductions[0].relay(k)
-    mlp_up(1)
-    mlp_down(1)
-    reductions[1].begin()
-    for k in (3, 1, 2, 0):
-        reductions[3].relay(k)
-    reductions[0].turn()
-    mlp_up(2)
-    mlp_down(2)
-    reductions[2].begin()
-    reductions[3].turn()
-    for k in (3, 1, 2, 0):
-        reductions[1].relay(k)
-    reductions[0].cross()
-    reductions[3].cross()
-    for k in (3, 1, 2, 0):
-        reductions[2].relay(k)
-    give_back(0)
-    give_back(3)
-    reductions[1].turn()
-    reductions[2].turn()
-    reductions[1].cross()
-    reductions[2].cross()
-    give_back(1)
-    give_back(2)
+
+    def enter(pair):
+        for u in pair:
+            rows_here(u)
+            gathers[u].begin()
+        both([gathers[u] for u in pair], ("across", 0))
+
+    def sideways(pair):
+        both([gathers[u] for u in pair], ("along",), ("across", 1), ("across", 2))
+
+    def gather_step(name, *given):
+        return lambda pair: both([gathers[u] for u in pair], (name, *given))
+
+    def reduce_step(name, *given):
+        return lambda pair: both([reductions[u] for u in pair], (name, *given))
+
+    def leave(pair):
+        for u in pair:
+            give_back(u)
+
+    steps = [
+        enter, sideways, gather_step("relay", 0), gather_step("turn"), gather_step("relay", 1), gather_step("relay", 2),
+        gather_step("relay", 3), mlp_up, mlp_down, reduce_step("begin"), reduce_step("relay", 3),
+        reduce_step("relay", 1), reduce_step("relay", 2), reduce_step("relay", 0), reduce_step("turn"),
+        reduce_step("cross"), leave,
+    ]
+    for i, step in ORDER:
+        steps[step](pairs[i])
 
     from_others = back.at[0 : count - 1]
     returned = remote(from_others, from_others, b_send.at[0], b_recv.at[0], (me, tp))
@@ -438,7 +442,6 @@
     inner = gate_weight.shape[2]
     heads = queries.shape[1]
     rows = 2 * count // UNITS
-    half = rows // 2
     groups = length // WINDOW
     peers = RING * RING
     dma = pltpu.SemaphoreType.DMA
@@ -464,10 +467,10 @@
             pltpu.VMEM((count, 2, width), BF16),
             pltpu.VMEM((UNITS * peers, rows, width), BF16),
             pltpu.VMEM((UNITS, RING, RING, rows, width), BF16),
-            pltpu.VMEM((UNITS, RING, 2, half, width), BF16),
+            pltpu.VMEM((UNITS, RING, 2, rows, width // 2), BF16),
             pltpu.VMEM((UNITS, RING, 2, rows, width), BF16),
             pltpu.VMEM((UNITS, RING, rows, width), BF16),
-            pltpu.VMEM((UNITS, 2, half, width), BF16),
+            pltpu.VMEM((UNITS, 2, rows, width // 2), BF16),
             pltpu.VMEM((UNITS, 2, rows, width), BF16),
             pltpu.VMEM((count, 2, width), BF16),
             pltpu.VMEM((count, 2, width), BF16),

time: 114 us -> 106 us (0.930)
  Pallas kernels: 112 us -> 104 us
    pallas_call x1, Pallas kernels: 112 us -> 104 us  [local(): pl.pallas_call(functools.partial(kernel, count), out_shape=jax.ShapeDtype...]
where the time goes in v4:
time: 106 us
  Pallas kernels  104 us (98%)
  other arithmetic  1.54 us (1%)
    pallas_call x1, Pallas kernels, local(): pl.pallas_call(functools.partial(kernel, count), out_shape=jax.ShapeDtype...  104 us

profile of v4, /device:TPU:1, one launch (start us, length us, event | category | flops | bytes accessed | tf_op | source)
XLA Modules:
  0.0 105.9 jit_solution(17008567371529734599)
XLA Ops:
  0.0 104.3 %layer.1 = f32[16,2048]{1,0:T(8,128)} custom-call(bf16[256,128]{1,0:T(8,128)(2,1)} %q_in.1, bf16[64,256]{1,0:T(8,128)(2,1)} %bitcast.9, bf16[64,256]{1,0:T(8,128)(2,1)} %bitcast.10, f32[2]{0:T(128)} %sink_in.1, bf16[2048,128]{1,0:T(8,128)(2,1)} %w_in.1, bf16[16,2048]{1,0:T(8,128)(2,1)} %res_in.1, f32[1,2048]{1,0:T(1,128)} %bitcast.11, s32[2,16]{1,0:T(2,128)} %bitcast.12, ...), custom_call_target="tpu_custom_call" | custom-call | tf_op jit(solution)/shard_map/layer/pallas_call | solution.py:454
  104.3 1.5 %convert_element_type.3 = bf16[16,2048]{1,0:T(8,128)(2,1)} convert(f32[16,2048]{1,0:T(8,128)} %layer.1) | non-fusion elementwise | flops 32768 | bytes 196608 | tf_op jit(solution)/shard_map/convert_element_type | solution.py:498

commit v5 on v4

--- a/solution.py
+++ b/solution.py
@@ -44,9 +44,9 @@
     q_in, kt_in, vt_in, sink_in, w_in, res_in, gain_in, routes_in, rw_in, wg_in, wu_in, wd_in,
     out_ref,
     q_ref, kt_ref, vt_ref, sink_ref, w_ref, res_ref, gain_ref, routes_ref, rw_ref, wg, wu, wd,
-    k_ext, v_ext, attn_all, cols, proj,
+    k_ext, v_ext, w_all, attended, shares, joined, rows_out, proj,
     sending, arrived, x_all, p_all, half_s, full_s, sums, half_f, full_f, back_send, back,
-    in_sem, h_send, h_recv, a_send, a_recv, o_send, o_recv, d_send, d_recv, b_send, b_recv, g_send, g_recv, r_send, r_recv,
+    in_sem, h_send, h_recv, w_send, w_recv, a_send, a_recv, s_send, s_recv, o_send, o_recv, d_send, d_recv, b_send, b_recv, g_send, g_recv, r_send, r_recv,
 ):
     me = lax.axis_index("sp")
     tp = lax.axis_index("tp")
@@ -55,8 +55,11 @@
     spot = {"x": tx, "y": ty}
     rows = 2 * count // UNITS
     per = count // UNITS
-    tokens, width = proj.shape
+    tokens, width = res_ref.shape
     length = q_ref.shape[0]
+    orders = [("x", "y"), ("y", "x")]
+    colors = range(2)
+    part = tokens // 2
     groups = length // WINDOW
 
     def shifted(pos, delta):
@@ -81,13 +84,13 @@
     lax.fori_loop(1, peers, greet_tp, 0)
 
     pairs = [
-        (kt_in, kt_ref), (vt_in, vt_ref), (q_in, q_ref), (sink_in, sink_ref), (routes_in, routes_ref), (rw_in, rw_ref),
-        (w_in, w_ref), (res_in, res_ref), (gain_in, gain_ref), (wg_in.at[0], wg), (wu_in.at[0], wu), (wd_in.at[0], wd),
+        (kt_in, kt_ref), (vt_in, vt_ref), (q_in, q_ref), (sink_in, sink_ref), (w_in, w_ref), (routes_in, routes_ref),
+        (rw_in, rw_ref), (res_in, res_ref), (gain_in, gain_ref), (wg_in.at[0], wg), (wu_in.at[0], wu), (wd_in.at[0], wd),
     ]
     loads = [pltpu.make_async_copy(src, dst, in_sem.at[i]) for i, (src, dst) in enumerate(pairs)]
     for copy in loads:
         copy.start()
-    for copy in loads[:4]:
+    for copy in loads[:5]:
         copy.wait()
     k_ext[:, WINDOW : WINDOW + length] = kt_ref[...]
     v_ext[:, WINDOW : WINDOW + length] = vt_ref[...]
@@ -102,11 +105,27 @@
             own.at[:, 0:WINDOW], ext.at[:, WINDOW + length : 2 * WINDOW + length], h_send.at[0], h_recv.at[0], (left, tp)
         ).start()
     halo = remote(k_ext, k_ext, h_send.at[0], h_recv.at[0], (me, tp))
+
+    core = lax.rem(me, 2)
+    mine = pl.ds(2 * core, 2)
+
+    def head_blocks(c, s):
+        return (s, mine) if c == 0 else (mine, s)
+
+    for c in colors:
+        second = orders[c][1]
+        s = spot[second]
+        for delta in (2, 1, -1):
+            remote(
+                w_ref.at[head_blocks(c, shifted(s, delta))], w_all.at[c, s, mine], w_send.at[0], w_recv.at[0],
+                near(second, delta),
+            ).start()
+        w_all[c, s, mine] = w_ref[head_blocks(c, s)]
     halo.wait_recv()
 
     class Gather:
-        def __init__(self, blocks, base, axes, cut, send_sem, recv_sem):
-            self.blocks, self.base, self.cut = blocks, base, cut
+        def __init__(self, blocks, base, axes, send_sem, recv_sem):
+            self.blocks, self.base = blocks, base
             self.first, self.second = axes
             self.f, self.s = spot[self.first], spot[self.second]
             self.send_sem, self.recv_sem = send_sem, recv_sem
@@ -118,9 +137,6 @@
             return self.blocks.at[self.place(s, k)]
 
         def part(self, ref, which):
-            if self.cut == 0:
-                h = ref.shape[0] // 2
-                return ref.at[which * h : (which + 1) * h]
             h = ref.shape[1] // 2
             return ref.at[:, which * h : (which + 1) * h]
 
@@ -159,9 +175,6 @@
 
         def complete(self):
             self.landed(7, self.blocks.at[0:RING])
-
-    orders = [("x", "y"), ("y", "x")]
-    attended = [Gather(attn_all, n * peers, orders[n], 0, a_send.at[0], a_recv.at[n]) for n in range(groups)]
 
     row_i = lax.broadcasted_iota(jnp.int32, (WINDOW, 3 * WINDOW), 0)
     col_j = lax.broadcasted_iota(jnp.int32, (WINDOW, 3 * WINDOW), 1)
@@ -179,14 +192,25 @@
             probs = jnp.exp(masked - top)
             denom = jnp.sum(probs, axis=-1, keepdims=True) + jnp.exp(sink - top)
             weights = (probs / denom).astype(BF16)
-            attn_all[attended[n].place(attended[n].s, 0), :, r * HEAD : (r + 1) * HEAD] = contract_last(
-                weights, v_ext[:, band]
-            ).astype(BF16)
-        attended[n].begin()
-    for part in attended:
-        part.across(0)
-
-    for copy in loads[4:9]:
+            output = contract_last(weights, v_ext[:, band]).reshape(WINDOW // tokens, tokens, HEAD)
+            half = WINDOW // 2
+            for c in colors:
+                attended[c, spot[orders[c][0]], n * half : (n + 1) * half, r * HEAD : (r + 1) * HEAD] = (
+                    output[:, c * part : (c + 1) * part].reshape(half, HEAD).astype(BF16)
+                )
+
+    for c in colors:
+        first = orders[c][0]
+        own = attended.at[c, spot[first]]
+        for delta in (2, 1, -1):
+            remote(own, own, a_send.at[c], a_recv.at[c], near(first, delta)).start()
+    fetched = w_all.at[0, 0 : RING - 1]
+    remote(fetched, fetched, w_send.at[0], w_recv.at[0], (me, tp)).wait_recv()
+    for c in colors:
+        half_blocks = w_all.at[c, :, mine]
+        remote(half_blocks, half_blocks, w_send.at[1], w_recv.at[1], (me + 1 - 2 * core, tp)).start()
+
+    for copy in loads[5:9]:
         copy.wait()
     t_row = lax.broadcasted_iota(jnp.int32, (tokens, tokens), 0)
     t_col = lax.broadcasted_iota(jnp.int32, (tokens, tokens), 1)
@@ -215,34 +239,48 @@
             for item in items:
                 getattr(item, name)(*given)
 
-    both(
-        attended, ("along",), ("across", 1), ("across", 2), ("relay", 0), ("turn",), ("relay", 1), ("relay", 2),
-        ("relay", 3), ("complete",),
-    )
-
-    for n in range(groups):
-        ys = [(t // RING, t % RING) if n == 0 else (t % RING, t // RING) for t in range(peers)]
-        joined = jnp.concatenate([attn_all[n * peers + i * RING + j] for i, j in ys], axis=1)
-        cols[n * WINDOW : (n + 1) * WINDOW, :] = jnp.dot(
-            joined, w_ref[...], preferred_element_type=F32
-        ).astype(BF16)
-    own_columns = pl.ds(pl.multiple_of(tp * WINDOW, WINDOW), WINDOW)
-
-    def rows_to(step, carry):
-        to = lax.rem(tp + step, peers)
-        remote(
-            cols.at[pl.ds(pl.multiple_of(to * tokens, tokens), tokens), :], proj.at[:, own_columns],
-            o_send.at[0], o_recv.at[0], (me, to),
-        ).start()
-        return carry
-
-    lax.fori_loop(1, peers, rows_to, 0)
-    proj[:, own_columns] = cols[pl.ds(pl.multiple_of(tp * tokens, tokens), tokens), :]
-    others = proj.at[:, 0 : (peers - 1) * WINDOW]
-    exchanged = remote(others, others, o_send.at[0], o_recv.at[0], (me, tp))
-    exchanged.wait_recv()
-
-    hidden_state = res_ref[...].astype(F32) + proj[...].astype(F32)
+    handed = w_all.at[0]
+    remote(handed, handed, w_send.at[1], w_recv.at[1], (me, tp)).wait_recv()
+    for c in colors:
+        arriving = attended.at[c, 0 : RING - 1]
+        remote(arriving, arriving, a_send.at[c], a_recv.at[c], (me, tp)).wait_recv()
+        heads = jnp.concatenate([attended[c, i] for i in range(RING)], axis=1)
+        for j in range(RING):
+            block = w_all[c, j].reshape(RING * WINDOW, WINDOW)
+            share = jnp.dot(heads, block, preferred_element_type=F32)
+            for t in range(peers):
+                s, f = (t // RING, t % RING) if c == 0 else (t % RING, t // RING)
+                shares[c, s, f * part : (f + 1) * part, j * WINDOW : (j + 1) * WINDOW] = share[
+                    t * part : (t + 1) * part
+                ].astype(BF16)
+        second = orders[c][1]
+        for delta, place in ((2, 2), (1, 0), (-1, 1)):
+            remote(
+                shares.at[c, shifted(spot[second], delta)], joined.at[c, place], s_send.at[c], s_recv.at[c],
+                near(second, delta),
+            ).start()
+    for c in colors:
+        first, second = orders[c]
+        f = spot[first]
+        remote(joined.at[c], joined.at[c], s_send.at[c], s_recv.at[c], (me, tp)).wait_recv()
+        total = shares[c, spot[second]].astype(F32)
+        for i in range(RING - 1):
+            total = total + joined[c, i].astype(F32)
+        rows_out[c] = total.reshape(RING, part, RING * WINDOW).astype(BF16)
+        for delta in (2, 1, -1):
+            remote(
+                rows_out.at[c, shifted(f, delta)], proj.at[c, f], o_send.at[c], o_recv.at[c], near(first, delta)
+            ).start()
+        proj[c, f] = rows_out[c, f]
+    for c in colors:
+        arriving = proj.at[c, 0 : RING - 1]
+        remote(arriving, arriving, o_send.at[c], o_recv.at[c], (me, tp)).wait_recv()
+    projected = []
+    for t in range(peers):
+        y, x = t // RING, t % RING
+        ends = [proj[0, x, :, y * WINDOW : (y + 1) * WINDOW], proj[1, y, :, x * WINDOW : (x + 1) * WINDOW]]
+        projected.append(jnp.concatenate([piece.astype(F32) for piece in ends], axis=0))
+    hidden_state = res_ref[...].astype(F32) + jnp.concatenate(projected, axis=1)
     inverse = lax.rsqrt(jnp.mean(hidden_state * hidden_state, axis=-1, keepdims=True) + EPS)
     normed = (hidden_state * inverse * gain_ref[...]).astype(BF16)
     slots = jnp.dot(placed, normed, preferred_element_type=F32).astype(BF16)
@@ -335,7 +373,7 @@
             return own + self.ff[0].astype(F32) + self.ff[1].astype(F32)
 
     axes = [orders[2 * u // UNITS] for u in range(UNITS)]
-    gathers = [Gather(x_all, u * peers, axes[u], 1, g_send.at[0], g_recv.at[u]) for u in range(UNITS)]
+    gathers = [Gather(x_all, u * peers, axes[u], g_send.at[0], g_recv.at[u]) for u in range(UNITS)]
     reductions = [Reduction(u, axes[u]) for u in range(UNITS)]
 
     def rows_here(u):
@@ -423,10 +461,15 @@
     returned.wait_send()
     dispatched = sending.at[0 : count - 1]
     remote(dispatched, dispatched, d_send.at[0], b_recv.at[0], (me, tp)).wait_send()
-    exchanged.wait_send()
     halo.wait_send()
-    sent = attn_all.at[0 : groups * (peers - 1)]
-    remote(sent, sent, a_send.at[0], b_recv.at[0], (me, tp)).wait_send()
+    remote(fetched, fetched, w_send.at[0], b_recv.at[0], (me, tp)).wait_send()
+    remote(handed, handed, w_send.at[1], b_recv.at[0], (me, tp)).wait_send()
+    for c in colors:
+        sent = attended.at[c, 0 : RING - 1]
+        remote(sent, sent, a_send.at[c], b_recv.at[0], (me, tp)).wait_send()
+        remote(joined.at[c], joined.at[c], s_send.at[c], b_recv.at[0], (me, tp)).wait_send()
+        sent = proj.at[c, 0 : RING - 1]
+        remote(sent, sent, o_send.at[c], b_recv.at[0], (me, tp)).wait_send()
     sent = x_all.at[0 : UNITS * (peers - 1)]
     remote(sent, sent, g_send.at[0], b_recv.at[0], (me, tp)).wait_send()
     remote(sent, sent, r_send.at[0], b_recv.at[0], (me, tp)).wait_send()
@@ -442,11 +485,10 @@
     inner = gate_weight.shape[2]
     heads = queries.shape[1]
     rows = 2 * count // UNITS
-    groups = length // WINDOW
     peers = RING * RING
     dma = pltpu.SemaphoreType.DMA
     given = (
-        queries, keys.T, values.T, sink_logit, out_weight, residual, norm_gain.reshape(1, width), routes.T,
+        queries, keys.T, values.T, sink_logit, out_weight.reshape(RING, RING, WINDOW, WINDOW), residual, norm_gain.reshape(1, width), routes.T,
         route_weights.T, jnp.swapaxes(gate_weight, 1, 2), jnp.swapaxes(up_weight, 1, 2), down_weight,
     )
     held = [pltpu.VMEM(a.shape, a.dtype) for a in given[:9]] + [pltpu.VMEM((inner, width), BF16)] * 3
@@ -460,9 +502,12 @@
             *held,
             pltpu.VMEM((kv, length + 2 * WINDOW), BF16),
             pltpu.VMEM((kv, length + 2 * WINDOW), BF16),
-            pltpu.VMEM((groups * peers, WINDOW, heads), BF16),
-            pltpu.VMEM((length, heads), BF16),
-            pltpu.VMEM((tokens, width), BF16),
+            pltpu.VMEM((2, RING, RING, WINDOW, WINDOW), BF16),
+            pltpu.VMEM((2, RING, length // 2, heads), BF16),
+            pltpu.VMEM((2, RING, RING * tokens // 2, RING * WINDOW), BF16),
+            pltpu.VMEM((2, RING - 1, RING * tokens // 2, RING * WINDOW), BF16),
+            pltpu.VMEM((2, RING, tokens // 2, RING * WINDOW), BF16),
+            pltpu.VMEM((2, RING, tokens // 2, RING * WINDOW), BF16),
             pltpu.VMEM((count, 2, width), BF16),
             pltpu.VMEM((count, 2, width), BF16),
             pltpu.VMEM((UNITS * peers, rows, width), BF16),
@@ -477,10 +522,14 @@
             dma((len(given),)),
             dma((1,)),
             dma((1,)),
-            dma((1,)),
-            dma((groups, 8)),
-            dma((1,)),
-            dma((1,)),
+            dma((2,)),
+            dma((2,)),
+            dma((2,)),
+            dma((2,)),
+            dma((2,)),
+            dma((2,)),
+            dma((2,)),
+            dma((2,)),
             dma((1,)),
             dma((UNITS,)),
             dma((1,)),

time: 106 us -> 99.5 us (0.939)
  Pallas kernels: 104 us -> 97.9 us
    pallas_call x1, Pallas kernels: 104 us -> 97.9 us  [local(): pl.pallas_call(functools.partial(kernel, count), out_shape=jax.ShapeDtype...]
where the time goes in v5:
time: 99.5 us; the launch traced here: 99.4 us
  Pallas kernels  97.9 us (98%)
  other arithmetic  1.54 us (2%)
    pallas_call x1, Pallas kernels, local(): pl.pallas_call(functools.partial(kernel, count), out_shape=jax.ShapeDtype...  97.9 us

profile of v5, /device:TPU:1, one launch (start us, length us, event | category | flops | bytes accessed | tf_op | source)
XLA Modules:
  0.0 99.4 jit_solution(17635535125595897982)
XLA Ops:
  0.0 97.9 %layer.1 = f32[16,2048]{1,0:T(8,128)} custom-call(bf16[256,128]{1,0:T(8,128)(2,1)} %q_in.1, bf16[64,256]{1,0:T(8,128)(2,1)} %bitcast.11, bf16[64,256]{1,0:T(8,128)(2,1)} %bitcast.12, f32[2]{0:T(128)} %sink_in.1, bf16[4,4,128,128]{3,2,1,0:T(8,128)(2,1)} %bitcast.10, bf16[16,2048]{1,0:T(8,128)(2,1)} %res_in.1, f32[1,2048]{1,0:T(1,128)} %bitcast.13, ...), custom_call_target="tpu_custom_call" | custom-call | tf_op jit(solution)/shard_map/layer/pallas_call | solution.py:496
  97.9 1.5 %convert_element_type.3 = bf16[16,2048]{1,0:T(8,128)(2,1)} convert(f32[16,2048]{1,0:T(8,128)} %layer.1) | non-fusion elementwise | flops 32768 | bytes 196608 | tf_op jit(solution)/shard_map/convert_element_type | solution.py:547

commit v6 on v5

--- a/solution.py
+++ b/solution.py
@@ -17,12 +17,12 @@
 UNITS = 8
 RING = 4
 ORDER = (
-    (0, 0), (0, 1), (1, 0), (0, 2), (0, 3), (0, 4), (0, 5), (1, 1), (2, 0), (0, 6), (1, 2), (1, 3), (3, 0), (2, 1),
-    (1, 4), (0, 7), (1, 5), (1, 6), (2, 2), (0, 8), (2, 3), (3, 1), (2, 4), (2, 5), (3, 2), (1, 7), (2, 6), (3, 3),
-    (1, 8), (1, 9), (3, 4), (0, 9), (3, 5), (2, 7), (3, 6), (1, 10), (2, 8), (2, 9), (1, 11), (1, 12), (1, 13),
-    (2, 10), (1, 14), (2, 11), (2, 12), (3, 7), (2, 13), (3, 8), (2, 14), (1, 15), (3, 9), (0, 10), (2, 15), (1, 16),
-    (3, 10), (3, 11), (3, 12), (3, 13), (2, 16), (3, 14), (0, 11), (0, 12), (0, 13), (0, 14), (3, 15), (0, 15),
-    (3, 16), (0, 16),
+    (0, 0), (0, 1), (0, 2), (0, 3), (1, 0), (0, 4), (0, 5), (0, 6), (1, 1), (2, 0), (1, 2), (1, 3), (1, 4), (3, 0),
+    (2, 1), (1, 5), (1, 6), (0, 7), (2, 2), (0, 8), (1, 7), (0, 9), (2, 3), (2, 4), (3, 1), (3, 2), (2, 5), (2, 6),
+    (3, 3), (1, 8), (2, 7), (3, 4), (1, 9), (3, 5), (1, 10), (3, 6), (0, 10), (2, 8), (1, 11), (3, 7), (2, 9),
+    (2, 10), (1, 12), (1, 13), (1, 14), (1, 15), (2, 11), (2, 12), (2, 13), (2, 14), (3, 8), (3, 9), (1, 16), (1, 17),
+    (2, 15), (3, 10), (0, 11), (1, 18), (2, 16), (2, 17), (3, 11), (3, 12), (3, 13), (0, 12), (0, 13), (3, 14),
+    (2, 18), (3, 15), (3, 16), (3, 17), (0, 14), (0, 15), (0, 16), (0, 17), (3, 18), (0, 18),
 )
 MESH = pl.DeviceIdType.MESH
 BF16 = jnp.bfloat16
@@ -70,25 +70,28 @@
             return (me, ty * RING + shifted(tx, delta))
         return (me, shifted(ty, delta) * RING + tx)
 
-    barrier = pltpu.get_barrier_semaphore()
-
-    def greet_sp(step, carry):
-        pl.semaphore_signal(barrier, inc=1, device_id=(lax.rem(me + step, count), tp), device_id_type=MESH)
-        return carry
-
-    def greet_tp(step, carry):
-        pl.semaphore_signal(barrier, inc=1, device_id=(me, lax.rem(tp + step, peers)), device_id_type=MESH)
-        return carry
-
-    lax.fori_loop(1, count, greet_sp, 0)
-    lax.fori_loop(1, peers, greet_tp, 0)
-
     pairs = [
         (kt_in, kt_ref), (vt_in, vt_ref), (q_in, q_ref), (sink_in, sink_ref), (w_in, w_ref), (routes_in, routes_ref),
         (rw_in, rw_ref), (res_in, res_ref), (gain_in, gain_ref), (wg_in.at[0], wg), (wu_in.at[0], wu), (wd_in.at[0], wd),
     ]
     loads = [pltpu.make_async_copy(src, dst, in_sem.at[i]) for i, (src, dst) in enumerate(pairs)]
-    for copy in loads:
+    for copy in loads[:5]:
+        copy.start()
+
+    barrier = pltpu.get_barrier_semaphore()
+
+    def greet_sp(step, carry):
+        pl.semaphore_signal(barrier, inc=1, device_id=(lax.rem(me + step, count), tp), device_id_type=MESH)
+        return carry
+
+    def greet_tp(step, carry):
+        pl.semaphore_signal(barrier, inc=1, device_id=(me, lax.rem(tp + step, peers)), device_id_type=MESH)
+        return carry
+
+    lax.fori_loop(1, count, greet_sp, 0)
+    lax.fori_loop(1, peers, greet_tp, 0)
+
+    for copy in loads[5:]:
         copy.start()
     for copy in loads[:5]:
         copy.wait()
@@ -121,11 +124,10 @@
                 near(second, delta),
             ).start()
         w_all[c, s, mine] = w_ref[head_blocks(c, s)]
-    halo.wait_recv()
 
     class Gather:
-        def __init__(self, blocks, base, axes, send_sem, recv_sem):
-            self.blocks, self.base = blocks, base
+        def __init__(self, blocks, base, axes, direct, send_sem, recv_sem):
+            self.blocks, self.base, self.direct = blocks, base, direct
             self.first, self.second = axes
             self.f, self.s = spot[self.first], spot[self.second]
             self.send_sem, self.recv_sem = send_sem, recv_sem
@@ -150,6 +152,8 @@
             own = self.block(self.s, 0)
             self.send(0, own, self.first, 1)
             self.send(1, own, self.first, -1)
+            if self.direct:
+                self.send(2, own, self.first, 2)
 
         def across(self, k):
             own = self.block(self.s, k)
@@ -159,17 +163,23 @@
         def along(self):
             low, high = self.block(self.s, 1), self.block(self.s, 2)
             self.landed(0, low)
-            self.send(2, self.part(low, 0), self.first, 1)
+            if not self.direct:
+                self.send(2, self.part(low, 0), self.first, 1)
             self.landed(1, high)
-            self.send(2, self.part(high, 1), self.first, -1)
+            if not self.direct:
+                self.send(2, self.part(high, 1), self.first, -1)
 
         def turn(self):
             self.landed(2, self.block(self.s, 3))
+            if self.direct:
+                self.send(7, self.block(self.s, 3), self.second, 2)
             self.across(3)
 
         def relay(self, k):
             low, high = self.block(shifted(self.s, -1), k), self.block(shifted(self.s, 1), k)
             self.landed(3 + k, self.blocks.at[0:2])
+            if self.direct and k == 3:
+                return
             self.send(7, self.part(low, 0), self.second, 1)
             self.send(7, self.part(high, 1), self.second, -1)
 
@@ -179,15 +189,25 @@
     row_i = lax.broadcasted_iota(jnp.int32, (WINDOW, 3 * WINDOW), 0)
     col_j = lax.broadcasted_iota(jnp.int32, (WINDOW, 3 * WINDOW), 1)
     close = (col_j >= row_i) & (col_j <= row_i + 2 * WINDOW)
-    for n in range(groups):
+    def part_scores(n, r, low, high):
         position = me * length + (n - 1) * WINDOW + col_j
         valid = close & (position >= 0) & (position < length * count)
+        query = q_ref[n * WINDOW : (n + 1) * WINDOW, r * HEAD : (r + 1) * HEAD]
+        keys = k_ext[:, n * WINDOW + low : n * WINDOW + high]
+        scores = jnp.dot(query, keys, preferred_element_type=F32) * HEAD ** (-0.5)
+        return jnp.where(valid[:, low:high], scores, NEGATIVE)
+
+    heads_here = [(n, r) for n in range(groups) for r in range(HEADS // KV_HEADS)]
+    own_range = [(WINDOW, 3 * WINDOW), (0, 2 * WINDOW)]
+    far_range = [(0, WINDOW), (2 * WINDOW, 3 * WINDOW)]
+    own_scores = {(n, r): part_scores(n, r, *own_range[n]) for n, r in heads_here}
+    halo.wait_recv()
+    for n in range(groups):
         band = slice(n * WINDOW, (n + 3) * WINDOW)
         for r in range(HEADS // KV_HEADS):
-            query = q_ref[n * WINDOW : (n + 1) * WINDOW, r * HEAD : (r + 1) * HEAD]
-            scores = jnp.dot(query, k_ext[:, band], preferred_element_type=F32) * HEAD ** (-0.5)
+            far = part_scores(n, r, *far_range[n])
+            masked = jnp.concatenate([far, own_scores[n, r]] if n == 0 else [own_scores[n, r], far], axis=1)
             sink = jnp.full((WINDOW, 1), sink_ref[r], F32)
-            masked = jnp.where(valid, scores, NEGATIVE)
             top = jnp.maximum(jnp.max(masked, axis=-1, keepdims=True), sink)
             probs = jnp.exp(masked - top)
             denom = jnp.sum(probs, axis=-1, keepdims=True) + jnp.exp(sink - top)
@@ -308,7 +328,8 @@
     arrived[0] = sending[me]
 
     class Reduction:
-        def __init__(self, unit, axes):
+        def __init__(self, unit, axes, direct):
+            self.direct = direct
             self.first, self.second = axes
             self.f, self.s = spot[self.first], spot[self.second]
             self.parts, self.hs, self.fs = p_all.at[unit], half_s.at[unit], full_s.at[unit]
@@ -351,30 +372,35 @@
         def turn(self):
             h = width // 2
             self.total[3] = self.summed(3).astype(BF16)
+            if self.direct:
+                self.send(10, self.total.at[3], self.ff.at[2], self.first, 2)
+                return
             self.send(8, self.total.at[3, :, 0:h], self.hf.at[0], self.first, 1)
             self.send(9, self.total.at[3, :, h:width], self.hf.at[1], self.first, -1)
 
-        def cross(self):
-            h = width // 2
-            high = self.summed(2)
-            self.landed(8, self.hf.at[0])
-            self.total[2, :, 0:h] = (high[:, 0:h] + self.hf[0].astype(F32)).astype(BF16)
-            self.total[2, :, h:width] = high[:, h:].astype(BF16)
-            self.send(10, self.total.at[2], self.ff.at[0], self.first, 1)
-            low = self.summed(1)
-            self.landed(9, self.hf.at[1])
-            self.total[1, :, 0:h] = low[:, 0:h].astype(BF16)
-            self.total[1, :, h:width] = (low[:, h:] + self.hf[1].astype(F32)).astype(BF16)
-            self.send(10, self.total.at[1], self.ff.at[1], self.first, -1)
+        def cross(self, k):
+            h, i = width // 2, 2 - k
+            block = self.summed(k)
+            halves = [block[:, 0:h], block[:, h:width]]
+            if not self.direct:
+                self.landed(8 + i, self.hf.at[i])
+                halves[i] = halves[i] + self.hf[i].astype(F32)
+            self.total[k, :, 0:h] = halves[0].astype(BF16)
+            self.total[k, :, h:width] = halves[1].astype(BF16)
+            self.send(10, self.total.at[k], self.ff.at[i], self.first, 1 - 2 * i)
 
         def finish(self):
             own = self.summed(0)
-            self.landed(10, self.ff)
-            return own + self.ff[0].astype(F32) + self.ff[1].astype(F32)
+            senders = 3 if self.direct else 2
+            self.landed(10, self.ff.at[0:senders])
+            for i in range(senders):
+                own = own + self.ff[i].astype(F32)
+            return own
 
     axes = [orders[2 * u // UNITS] for u in range(UNITS)]
-    gathers = [Gather(x_all, u * peers, axes[u], g_send.at[0], g_recv.at[u]) for u in range(UNITS)]
-    reductions = [Reduction(u, axes[u]) for u in range(UNITS)]
+    straight = (pairs[0], pairs[0] + pairs[3])
+    gathers = [Gather(x_all, u * peers, axes[u], u in straight[0], g_send.at[0], g_recv.at[u]) for u in range(UNITS)]
+    reductions = [Reduction(u, axes[u], u in straight[1]) for u in range(UNITS)]
 
     def rows_here(u):
         first = 1 if u == 0 else 0
@@ -428,8 +454,8 @@
             gathers[u].begin()
         both([gathers[u] for u in pair], ("across", 0))
 
-    def sideways(pair):
-        both([gathers[u] for u in pair], ("along",), ("across", 1), ("across", 2))
+    def blocks_across(pair):
+        both([gathers[u] for u in pair], ("across", 1), ("across", 2))
 
     def gather_step(name, *given):
         return lambda pair: both([gathers[u] for u in pair], (name, *given))
@@ -442,10 +468,10 @@
             give_back(u)
 
     steps = [
-        enter, sideways, gather_step("relay", 0), gather_step("turn"), gather_step("relay", 1), gather_step("relay", 2),
-        gather_step("relay", 3), mlp_up, mlp_down, reduce_step("begin"), reduce_step("relay", 3),
+        enter, gather_step("along"), blocks_across, gather_step("relay", 0), gather_step("turn"), gather_step("relay", 1),
+        gather_step("relay", 2), gather_step("relay", 3), mlp_up, mlp_down, reduce_step("begin"), reduce_step("relay", 3),
         reduce_step("relay", 1), reduce_step("relay", 2), reduce_step("relay", 0), reduce_step("turn"),
-        reduce_step("cross"), leave,
+        reduce_step("cross", 2), reduce_step("cross", 1), leave,
     ]
     for i, step in ORDER:
         steps[step](pairs[i])
@@ -516,7 +542,7 @@
             pltpu.VMEM((UNITS, RING, 2, rows, width), BF16),
             pltpu.VMEM((UNITS, RING, rows, width), BF16),
             pltpu.VMEM((UNITS, 2, rows, width // 2), BF16),
-            pltpu.VMEM((UNITS, 2, rows, width), BF16),
+            pltpu.VMEM((UNITS, 3, rows, width), BF16),
             pltpu.VMEM((count, 2, width), BF16),
             pltpu.VMEM((count, 2, width), BF16),
             dma((len(given),)),

time: 99.5 us -> 98.1 us (0.986)
  Pallas kernels: 97.9 us -> 96.4 us
    pallas_call x1, Pallas kernels: 97.9 us -> 96.4 us  [local(): pl.pallas_call(functools.partial(kernel, count), out_shape=jax.ShapeDtype...]
where the time goes in v6:
time: 98.1 us; the launch traced here: 97.9 us
  Pallas kernels  96.4 us (98%)
  other arithmetic  1.54 us (2%)
    pallas_call x1, Pallas kernels, local(): pl.pallas_call(functools.partial(kernel, count), out_shape=jax.ShapeDtype...  96.4 us

profile of v6, /device:TPU:1, one launch (start us, length us, event | category | flops | bytes accessed | tf_op | source)
XLA Modules:
  0.0 97.9 jit_solution(1217225958727395420)
XLA Ops:
  0.0 96.4 %layer.1 = f32[16,2048]{1,0:T(8,128)} custom-call(bf16[256,128]{1,0:T(8,128)(2,1)} %q_in.1, bf16[64,256]{1,0:T(8,128)(2,1)} %bitcast.11, bf16[64,256]{1,0:T(8,128)(2,1)} %bitcast.12, f32[2]{0:T(128)} %sink_in.1, bf16[4,4,128,128]{3,2,1,0:T(8,128)(2,1)} %bitcast.10, bf16[16,2048]{1,0:T(8,128)(2,1)} %res_in.1, f32[1,2048]{1,0:T(1,128)} %bitcast.13, ...), custom_call_target="tpu_custom_call" | custom-call | tf_op jit(solution)/shard_map/layer/pallas_call | solution.py:522
  96.4 1.5 %convert_element_type.3 = bf16[16,2048]{1,0:T(8,128)(2,1)} convert(f32[16,2048]{1,0:T(8,128)} %layer.1) | non-fusion elementwise | flops 32768 | bytes 196608 | tf_op jit(solution)/shard_map/convert_element_type | solution.py:573
